TPU v7x, 32 devices: a whole 2x2x4 slice. The times are simulated.
32 devices in a mesh: ep: 16 (over z, y, x), tp: 2 (over core).
Axes of the slice: x: 2, y: 2, z: 4, core: 2. Of those that a mesh axis runs over, the one named last changes fastest.
Arguments:
- tokens: bfloat16 [256, 2048], P('ep'), may hold values from -6 to 6
- lengths: int32 [256], P('ep'), may hold values from 1024 to 8191
- prior_state: float32 [256, 16, 64, 64], P('ep', 'tp'), may hold values from -2 to 2
- mix_gain: float32 [2048], replicated, may hold values from 0.1 to 1.9
- post_gain: float32 [2048], replicated, may hold values from 0.1 to 1.9
- ffn_gain: float32 [2048], replicated, may hold values from 0.1 to 1.9
- out_gain: float32 [2048], replicated, may hold values from 0.1 to 1.9
- query_weight: bfloat16 [2048, 1024], P('ep', 'tp'), may hold values from -0.125 to 0.125
- key_weight: bfloat16 [2048, 1024], P('ep', 'tp'), may hold values from -0.125 to 0.125
- value_weight: bfloat16 [2048, 1024], P('ep', 'tp'), may hold values from -0.125 to 0.125
- gate_weight: bfloat16 [2048, 1024], P('ep', 'tp'), may hold values from -0.125 to 0.125
- out_weight: bfloat16 [1024, 2048], P('tp', 'ep'), may hold values from -0.1875 to 0.1875
- routes: int32 [256, 6], P('ep'), may hold values from 0 to 15, all different within a row; in each aligned block of 16 rows (0 to 15, 16 to 31, ...) at most 8 rows name the same one
- route_gates: float32 [256, 6], P('ep'), may hold values from 0.1 to 0.9
- expert_gate: bfloat16 [16, 2048, 512], P('ep', None, 'tp'), may hold values from -0.125 to 0.125
- expert_up: bfloat16 [16, 2048, 512], P('ep', None, 'tp'), may hold values from -0.125 to 0.125
- expert_down: bfloat16 [16, 512, 2048], P('ep', 'tp'), may hold values from -0.25 to 0.25
- shared_gate: bfloat16 [2048, 512], P(None, 'tp'), may hold values from -0.125 to 0.125
- shared_up: bfloat16 [2048, 512], P(None, 'tp'), may hold values from -0.125 to 0.125
- shared_down: bfloat16 [512, 2048], P('tp'), may hold values from -0.25 to 0.25
Outputs:
- result: bfloat16 [256, 2048], P('ep')
- new_state: float32 [256, 16, 64, 64], P('ep', 'tp')
Inputs may be any that keep to these rules, and one draw needn't show every extreme that they name: `routes`: each row names 6 different experts. In the rows of one device (aligned blocks of 16 rows) no expert is named more than 8 times, and in every draw some expert is named exactly 8 times in some block.
All inputs are finite; a program needn't handle non-finite values.
Results may differ from a plain program's by a relative error of at most 0.02.
Values may be sent and summed in bfloat16 or wider, within the bound.
A program may use at most 128 MiB of HBM per device.

v0:
```python
import jax
import jax.numpy as jnp
from jax import lax
from jax.sharding import PartitionSpec as P

HEAD = 64
HEADS = 16


EPS = 1e-06
THETA = 10000.0


def rounded(values):
    return lax.optimization_barrier(values.astype(jnp.bfloat16)).astype(jnp.float32)


def scaled_rows(values, gain_row):
    widened = values.astype(jnp.float32)
    return widened * lax.rsqrt(jnp.mean(widened * widened, axis=-1, keepdims=True) + EPS) * gain_row


def rotate(vectors, lengths):
    half_dim = vectors.shape[-1] // 2
    frequency = THETA ** (-jnp.arange(half_dim, dtype=jnp.float32) / half_dim)
    angles = lengths.astype(jnp.float32)[:, None] * frequency[None, :]
    cosine = jnp.cos(angles)[:, None, :]
    sine_part = jnp.sin(angles)[:, None, :]
    leading = vectors[..., :half_dim]
    trailing = vectors[..., half_dim:]
    return jnp.concatenate(
        [leading * cosine - trailing * sine_part, trailing * cosine + leading * sine_part], axis=-1
    )


def decay_table(head_count):
    head_order = jnp.arange(head_count, dtype=jnp.float32)
    return 1.0 - jnp.exp2(-5.0 - 7.0 * head_order / (head_count - 1))


def retain(queries, keys_new, values, out_gate, prior_state, lengths, decays):
    seq_count = queries.shape[0]
    head_count = decays.shape[0]
    layout = (seq_count, head_count, HEAD)
    rot_query = rotate(queries.astype(jnp.float32).reshape(layout), lengths)
    rot_key = rotate(keys_new.astype(jnp.float32).reshape(layout), lengths) * HEAD ** (-0.5)
    wide_values = values.astype(jnp.float32).reshape(layout)
    from_state = jnp.einsum(
        "shd,shde->she", rot_query, prior_state, precision=lax.Precision.HIGHEST
    )
    self_term = jnp.sum(rot_query * rot_key, axis=-1, keepdims=True)
    read_out = decays[None, :, None] * from_state + self_term * wide_values
    new_state = (
        decays[None, :, None, None] * prior_state
        + rot_key[..., :, None] * wide_values[..., None, :]
    )
    normed = read_out * lax.rsqrt(jnp.mean(read_out * read_out, axis=-1, keepdims=True) + EPS)
    gated_rows = normed.reshape(seq_count, head_count * HEAD) * jax.nn.silu(
        out_gate.astype(jnp.float32)
    )
    return (gated_rows.astype(jnp.bfloat16), new_state)


def on_device(
    tokens,
    lengths,
    prior_state,
    mix_gain,
    post_gain,
    ffn_gain,
    out_gain,
    query_weight,
    key_weight,
    value_weight,
    gate_weight,
    out_weight,
    routes,
    route_gates,
    expert_gate,
    expert_up,
    expert_down,
    shared_gate,
    shared_up,
    shared_down,
):
    seq_here = tokens.shape[0]
    model_width = tokens.shape[1]
    local_cols = query_weight.shape[1]
    normed = scaled_rows(tokens, mix_gain).astype(jnp.bfloat16)
    features = lax.all_to_all(normed, "ep", split_axis=1, concat_axis=0, tiled=True)
    joined = jnp.concatenate((query_weight, key_weight, value_weight, gate_weight), axis=1)
    summed = lax.psum_scatter(
        jnp.dot(features, joined, preferred_element_type=jnp.float32),
        "ep",
        scatter_dimension=0,
        tiled=True,
    )
    projected = tuple((summed[:, role * local_cols : (role + 1) * local_cols] for role in range(4)))
    queries, keys_new, values, out_gate = tuple(
        (member.astype(jnp.bfloat16) for member in projected)
    )
    heads_here = local_cols // HEAD
    decays = lax.dynamic_slice_in_dim(
        decay_table(HEADS), lax.axis_index("tp") * heads_here, heads_here, 0
    )
    retained, new_state = retain(queries, keys_new, values, out_gate, prior_state, lengths, decays)
    column_part = jnp.dot(
        lax.all_gather(retained, "ep", axis=0, tiled=True),
        out_weight,
        preferred_element_type=jnp.float32,
    ).astype(jnp.bfloat16)
    partial_mix = lax.all_to_all(column_part, "ep", split_axis=0, concat_axis=1, tiled=True).astype(
        jnp.float32
    )
    mixed_sum = rounded(
        lax.psum(rounded(partial_mix).astype(jnp.bfloat16), "tp").astype(jnp.float32)
    )
    middle = rounded(tokens.astype(jnp.float32) + scaled_rows(mixed_sum, post_gain))
    moe_in = scaled_rows(middle, ffn_gain).astype(jnp.bfloat16)
    experts_all = lax.axis_size("ep")
    topk_here = routes.shape[1]
    capacity = seq_here * topk_here // experts_all + 2
    slot_count = experts_all * capacity
    flat_routes = routes.reshape(-1)
    onehot = (flat_routes[:, None] == jnp.arange(experts_all, dtype=jnp.int32)[None, :]).astype(
        jnp.int32
    )
    earlier = jnp.cumsum(onehot, axis=0) - onehot
    ranks = jnp.sum(earlier * onehot, axis=1)
    slot_ids = flat_routes * capacity + ranks
    placing = (jnp.arange(slot_count, dtype=jnp.int32)[:, None] == slot_ids[None, :]).reshape(
        slot_count, seq_here, topk_here
    )
    dispatch_rows = jnp.any(placing, axis=2).astype(jnp.bfloat16)
    combine = jnp.sum(
        jnp.where(placing, route_gates[None, :, :], jnp.zeros((), jnp.float32)), axis=2
    ).T
    outgoing = jnp.dot(dispatch_rows, moe_in, preferred_element_type=jnp.float32).astype(
        jnp.bfloat16
    )
    outgoing = outgoing.reshape(experts_all, capacity, model_width)
    gate_local = expert_gate[0]
    up_local = expert_up[0]
    down_local = expert_down[0]
    arrived = lax.all_to_all(outgoing, "ep", split_axis=0, concat_axis=0, tiled=True)
    sources = arrived.shape[0]
    held_slots = arrived.shape[1]
    flat_in = arrived.reshape(sources * held_slots, model_width)
    hidden = (
        jax.nn.silu(jnp.dot(flat_in, gate_local, preferred_element_type=jnp.float32))
        * jnp.dot(flat_in, up_local, preferred_element_type=jnp.float32)
    ).astype(jnp.bfloat16)
    partial_out = rounded(jnp.dot(hidden, down_local, preferred_element_type=jnp.float32))
    expert_sum = lax.psum(partial_out.astype(jnp.bfloat16), "tp")
    returned = lax.all_to_all(
        expert_sum.reshape(sources, held_slots, -1), "ep", split_axis=0, concat_axis=0, tiled=True
    )
    back_rows = returned.reshape(slot_count, -1).astype(jnp.float32)
    routed = jnp.dot(combine, back_rows, precision=lax.Precision.HIGHEST)
    shared_hidden = (
        jax.nn.silu(jnp.dot(moe_in, shared_gate, preferred_element_type=jnp.float32))
        * jnp.dot(moe_in, shared_up, preferred_element_type=jnp.float32)
    ).astype(jnp.bfloat16)
    shared_part = rounded(jnp.dot(shared_hidden, shared_down, preferred_element_type=jnp.float32))
    shared_out = lax.psum(shared_part.astype(jnp.bfloat16), "tp")
    mixture = shared_out.astype(jnp.float32) + routed
    result = (middle + scaled_rows(mixture, out_gain)).astype(jnp.bfloat16)
    return (result, new_state)


def solution(mesh):
    return jax.shard_map(
        on_device,
        mesh=mesh,
        in_specs=(
            P("ep", None),
            P("ep"),
            P("ep", "tp", None, None),
            P(),
            P(),
            P(),
            P(),
            P("ep", "tp"),
            P("ep", "tp"),
            P("ep", "tp"),
            P("ep", "tp"),
            P("tp", "ep"),
            P("ep", None),
            P("ep", None),
            P("ep", None, "tp"),
            P("ep", None, "tp"),
            P("ep", "tp", None),
            P(None, "tp"),
            P(None, "tp"),
            P("tp", None),
        ),
        out_specs=(P("ep", None), P("ep", "tp", None, None)),
        check_vma=False,
    )
```

profile of v0, /device:TPU:0, one launch (start us, length us, event | category | flops | bytes accessed | tf_op | source)
XLA Modules:
  0.0 254.3 jit_solution(6704595756294250518)
XLA Ops:
  7.2 0.0 copy-start
  7.2 0.0 copy-start.10
  7.2 0.0 copy-start.6
  7.2 0.0 reduce-scatter.2.cloned.1.call-start
  7.2 1.0 fusion.25
  8.3 0.9 copy_bitcast_fusion.1
  9.2 15.7 %all_to_all.48 = bf16[16,16,128]{2,0,1:T(8,128)(2,1)S(1)} all-to-all(bf16[16,16,128]{2,0,1:T(8,128)(2,1)S(1)} %copy_bitcast_fusion.1), channel_id=1, replica_groups=mesh['ep'=16,'tp'=2] {'ep'}, dimensions={1} | all-to-all | bytes 131072 | tf_op jit(solution)/shard_map/all_to_all | solution.py:90
  24.9 2.8 %fusion.11 = f32[256,2048]{1,0:T(8,128)} fusion(bf16[256,128]{1,0:T(8,128)(2,1)S(1)} %bitcast.57, bf16[128,512]{1,0:T(8,128)(2,1)} %param.30, bf16[128,512]{1,0:T(8,128)(2,1)} %param.29, bf16[128,512]{1,0:T(8,128)(2,1)} %param.28, bf16[128,512]{1,0:T(8,128)(2,1)} %param.27), kind=kOutput, calls=%fused_computation.18 | convolution fusion | flops 136314880 | bytes 2686976 | tf_op jit(solution)/shard_map/dot_general | solution.py:93
  27.7 0.0 reduce-scatter.2.cloned.1.call-update
  27.8 0.0 copy-start.2
  27.8 0.0 copy-start.7
  27.8 0.0 copy-start.4
  27.8 0.0 copy-done.6
  27.8 0.1 copy.38
  27.9 0.1 eq.30
  28.0 0.1 fusion.40
  28.1 0.1 reduce_window_sum.11
  28.2 0.2 select_reduce_fusion.1
  28.4 0.1 reduce_sum.80
  28.5 0.1 copy.39
  28.6 0.1 dynamic_slice.3
  28.7 0.1 multiply_cosine_fusion
  28.8 77.1 %reduce-scatter.2.cloned.1.call-done = f32[16,2048]{1,0:T(8,128)} async-done(((f32[256,2048]{1,0:T(8,128)}), f32[16,2048]{1,0:T(8,128)}) %reduce-scatter.2.cloned.1.call-update) | async-done | bytes 131088 | tf_op jit(solution)/shard_map/reduce_scatter | solution.py:92
  105.9 0.9 convert.9
  106.8 0.1 reshape.191
  106.9 0.1 reshape.193
  107.0 0.1 reshape.189
  107.1 0.1 multiply_subtract_fusion
  107.2 0.1 pad_maximum_fusion
  107.3 5.3 %fusion.62 = f32[16,8,1,64]{3,2,1,0:T(1,128)S(1)} fusion(f32[16,8,64,1]{2,3,1,0:T(1,128)S(1)} %bitcast.55, f32[16,8,64,64]{3,2,1,0:T(8,128)} %param.22), kind=kOutput, calls=%fused_computation.103 | convolution fusion | flops 6291456 | bytes 2162688 | tf_op jit(solution)/shard_map/shd,shde->she/dot_general | solution.py:48
  112.6 0.2 multiply_reduce_fusion.1
  112.8 0.1 broadcast_multiply_fusion
  112.9 0.0 copy-start.1
  112.9 0.1 reshape.183
  113.0 38.2 %all_gather.3 = bf16[256,512]{1,0:T(8,128)(2,1)S(1)} all-gather(bf16[16,512]{1,0:T(8,128)(2,1)S(1)} %fusion.46), channel_id=1, replica_groups=mesh['ep'=16,'tp'=2] {'ep'}, dimensions={0}, use_global_device_ids=true | all-gather | bytes 278528 | tf_op jit(solution)/shard_map/all_gather | solution.py:108
  151.2 0.8 convolution_convert_fusion.3
  152.1 3.5 %all-to-all-start.1 = ((bf16[16,16,128]{2,1,0:T(8,128)(2,1)}), bf16[16,16,128]{2,1,0:T(8,128)(2,1)S(1)}, u32[]{:S(2)}, u32[]{:S(2)}) async-start(bf16[16,16,128]{2,1,0:T(8,128)(2,1)} %bitcast.6), calls=%async_computation.2 | async-start | bytes 131072 | tf_op jit(solution)/shard_map/all_to_all | solution.py:112
  155.6 0.0 all-reduce.4.cloned.1.call-start
  155.6 7.4 %all-to-all-done.1 = bf16[16,16,128]{2,1,0:T(8,128)(2,1)S(1)} async-done(((bf16[16,16,128]{2,1,0:T(8,128)(2,1)}), bf16[16,16,128]{2,1,0:T(8,128)(2,1)S(1)}, u32[]{:S(2)}, u32[]{:S(2)}) %all-to-all-start.1) | async-done | bytes 65568 | tf_op jit(solution)/shard_map/all_to_all | solution.py:112
  163.1 0.6 copy_bitcast_fusion
  163.7 0.0 all-reduce.4.cloned.1.call-update
  163.7 0.1 fusion.41
  163.8 14.5 %all-reduce.4.cloned.1.call-done = bf16[16,2048]{1,0:T(8,128)(2,1)} async-done(((bf16[16,2048]{1,0:T(8,128)(2,1)}), bf16[16,2048]{1,0:T(8,128)(2,1)}) %all-reduce.4.cloned.1.call-update) | async-done | bytes 65552 | tf_op jit(solution)/shard_map/psum | solution.py:116
  178.3 1.0 fusion.23
  179.3 0.0 copy-done.7
  179.3 0.9 fusion.28
  180.2 0.1 fusion.29
  180.4 1.1 fusion.1
  181.5 6.8 %all-to-all-start.2 = ((bf16[16,8,2048]{2,1,0:T(8,128)(2,1)}), bf16[16,8,2048]{2,1,0:T(8,128)(2,1)S(1)}, u32[]{:S(2)}, u32[]{:S(2)}) async-start(bf16[16,8,2048]{2,1,0:T(8,128)(2,1)} %fusion.1), calls=%async_computation.3 | async-start | bytes 1048576 | tf_op jit(solution)/shard_map/all_to_all | solution.py:145
  188.4 0.0 all-reduce.6.cloned.1.call-start
  188.4 1.5 fusion.60
  189.9 3.0 %convolution_convert_fusion.2 = bf16[16,2048]{1,0:T(8,128)(2,1)} fusion(bf16[256,2048]{1,0:T(8,128)(2,1)} %param.39, bf16[2048,256]{1,0:T(8,128)(2,1)} %param.38, f32[16,256]{1,0:T(8,128)S(1)} %fusion.60, bf16[16,2048]{1,0:T(8,128)(2,1)S(1)} %fusion.28, f32[2048]{0:T(1024)S(1)} %copy-done.4, f32[16]{0:T(128)S(1)} %add_rsqrt_fusion.2), kind=kOutput, calls=%fused_computation.6 | convolution fusion | flops 33742848 | bytes 2252864 | tf_op jit(solution)/shard_map/dot_general | solution.py:164
  192.9 10.9 %all-to-all-done.2 = bf16[16,8,2048]{2,1,0:T(8,128)(2,1)S(1)} async-done(((bf16[16,8,2048]{2,1,0:T(8,128)(2,1)}), bf16[16,8,2048]{2,1,0:T(8,128)(2,1)S(1)}, u32[]{:S(2)}, u32[]{:S(2)}) %all-to-all-start.2) | async-done | bytes 524320 | tf_op jit(solution)/shard_map/all_to_all | solution.py:145
  203.8 1.5 fusion.9
  205.4 1.6 convolution_convert_fusion
  207.0 0.0 all-reduce.6.cloned.1.call-update
  207.0 17.3 %all-reduce.6.cloned.1.call-done = (bf16[16,8,2048]{2,1,0:T(8,128)(2,1)}, bf16[16,2048]{1,0:T(8,128)(2,1)}) async-done(((bf16[16,8,2048]{2,1,0:T(8,128)(2,1)}, bf16[16,2048]{1,0:T(8,128)(2,1)}), (bf16[16,8,2048]{2,1,0:T(8,128)(2,1)}, bf16[16,2048]{1,0:T(8,128)(2,1)})) %all-reduce.6.cloned.1.call-update) | async-done | bytes 589840 | tf_op jit(solution)/shard_map/psum | solution.py:154
  224.3 6.8 %all-to-all-start.3 = ((bf16[16,8,2048]{2,1,0:T(8,128)(2,1)}), bf16[16,8,2048]{2,1,0:T(8,128)(2,1)S(1)}, u32[]{:S(2)}, u32[]{:S(2)}) async-start(bf16[16,8,2048]{2,1,0:T(8,128)(2,1)} %get-tuple-element.2), calls=%async_computation.4 | async-start | bytes 1048576 | tf_op jit(solution)/shard_map/all_to_all | solution.py:155
  231.1 0.1 select_reduce_fusion
  231.2 0.0 copy-start.8
  231.2 4.3 %multiply_add_fusion = f32[16,8,64,64]{3,2,1,0:T(8,128)} fusion(f32[16,8,64,64]{3,2,1,0:T(8,128)} %param.22, f32[16,8,64]{2,1,0:T(8,128)S(1)} %reshape.193, f32[16,8,64]{2,1,0:T(8,128)S(1)} %get-tuple-element.20, f32[8]{0:T(128)S(1)} %dynamic_slice.3), kind=kLoop, calls=%fused_computation.1 | loop fusion | flops 1572864 | bytes 4259872 | tf_op jit(solution)/shard_map/add | solution.py:54
  235.5 11.1 %all-to-all-done.3 = bf16[16,8,2048]{2,1,0:T(8,128)(2,1)S(1)} async-done(((bf16[16,8,2048]{2,1,0:T(8,128)(2,1)}), bf16[16,8,2048]{2,1,0:T(8,128)(2,1)S(1)}, u32[]{:S(2)}, u32[]{:S(2)}) %all-to-all-start.3) | async-done | bytes 524320 | tf_op jit(solution)/shard_map/all_to_all | solution.py:155
  246.6 0.4 multiply_reduce_fusion
  247.0 0.7 fusion.32
  (23 shorter events, 0.1 us)
Async XLA Ops:
  7.2 198.2 %copy-start = (bf16[1,256,2048]{2,1,0:T(8,128)(2,1)S(1)}, bf16[1,256,2048]{2,1,0:T(8,128)(2,1)}, u32[]{:S(2)}) copy-start(bf16[1,256,2048]{2,1,0:T(8,128)(2,1)} %param.36) | copy-start | bytes 3145732
  7.2 20.6 %copy-start.10 = (s32[16]{0:T(128)S(1)}, s32[16]{0:T(128)}, u32[]{:S(2)}) copy-start(s32[16]{0:T(128)} %param.21) | copy-start | bytes 196
  7.2 20.6 %copy-start.6 = (s32[16,6]{0,1:T(8,128)S(1)}, s32[16,6]{0,1:T(8,128)}, u32[]{:S(2)}) copy-start(s32[16,6]{0,1:T(8,128)} %param.32) | copy-start | bytes 1156
  7.2 98.7 %reduce-scatter.2.cloned.1.call-start = ((), (), s32[]{:S(2)}) async-start(), calls=%async_computation.5 | async-start | bytes 2228224 | tf_op jit(solution)/shard_map/reduce_scatter | solution.py:92
  27.7 123.5 %copy-start.3 = (bf16[512,128]{1,0:T(8,128)(2,1)S(1)}, bf16[512,128]{1,0:T(8,128)(2,1)}, u32[]{:S(2)}) copy-start(bf16[512,128]{1,0:T(8,128)(2,1)} %param.31) | copy-start | bytes 393220
  27.8 151.5 %copy-start.2 = (bf16[16,2048]{1,0:T(8,128)(2,1)S(1)}, bf16[16,2048]{1,0:T(8,128)(2,1)}, u32[]{:S(2)}) copy-start(bf16[16,2048]{1,0:T(8,128)(2,1)} %param.20) | copy-start | bytes 196612
  27.8 151.5 %copy-start.7 = (f32[2048]{0:T(1024)S(1)}, f32[2048]{0:T(1024)}, u32[]{:S(2)}) copy-start(f32[2048]{0:T(1024)} %param.24) | copy-start | bytes 24580
  27.8 152.6 %copy-start.4 = (f32[2048]{0:T(1024)S(1)}, f32[2048]{0:T(1024)}, u32[]{:S(2)}) copy-start(f32[2048]{0:T(1024)} %param.25) | copy-start | bytes 24580
  112.9 92.5 %copy-start.1 = (bf16[1,2048,256]{2,1,0:T(8,128)(2,1)S(1)}, bf16[1,2048,256]{2,1,0:T(8,128)(2,1)}, u32[]{:S(2)}) copy-start(bf16[1,2048,256]{2,1,0:T(8,128)(2,1)} %param.35) | copy-start | bytes 3145732
  152.1 11.0 %all-to-all-start.1 = ((bf16[16,16,128]{2,1,0:T(8,128)(2,1)}), bf16[16,16,128]{2,1,0:T(8,128)(2,1)S(1)}, u32[]{:S(2)}, u32[]{:S(2)}) async-start(bf16[16,16,128]{2,1,0:T(8,128)(2,1)} %bitcast.6), calls=%async_computation.2 | async-start | bytes 131072 | tf_op jit(solution)/shard_map/all_to_all | solution.py:112
  155.6 22.7 %all-reduce.4.cloned.1.call-start = ((), (), s32[]{:S(2)}) async-start(), calls=%async_computation.6 | async-start | bytes 131072 | tf_op jit(solution)/shard_map/psum | solution.py:116
  181.5 22.3 %all-to-all-start.2 = ((bf16[16,8,2048]{2,1,0:T(8,128)(2,1)}), bf16[16,8,2048]{2,1,0:T(8,128)(2,1)S(1)}, u32[]{:S(2)}, u32[]{:S(2)}) async-start(bf16[16,8,2048]{2,1,0:T(8,128)(2,1)} %fusion.1), calls=%async_computation.3 | async-start | bytes 1048576 | tf_op jit(solution)/shard_map/all_to_all | solution.py:145
  188.4 35.9 %all-reduce.6.cloned.1.call-start = ((), (), s32[]{:S(2)}) async-start(), calls=%async_computation.7 | async-start | bytes 1179648 | tf_op jit(solution)/shard_map/psum | solution.py:154
  189.9 41.2 %copy-start.9 = (f32[16,6]{0,1:T(8,128)S(1)}, f32[16,6]{0,1:T(8,128)}, u32[]{:S(2)}) copy-start(f32[16,6]{0,1:T(8,128)} %param.33) | copy-start | bytes 1156
  224.3 22.3 %all-to-all-start.3 = ((bf16[16,8,2048]{2,1,0:T(8,128)(2,1)}), bf16[16,8,2048]{2,1,0:T(8,128)(2,1)S(1)}, u32[]{:S(2)}, u32[]{:S(2)}) async-start(bf16[16,8,2048]{2,1,0:T(8,128)(2,1)} %get-tuple-element.2), calls=%async_computation.4 | async-start | bytes 1048576 | tf_op jit(solution)/shard_map/all_to_all | solution.py:155
  231.2 15.4 %copy-start.5 = (bf16[16,2048]{1,0:T(8,128)(2,1)S(1)}, bf16[16,2048]{1,0:T(8,128)(2,1)}, u32[]{:S(2)}) copy-start(bf16[16,2048]{1,0:T(8,128)(2,1)} %get-tuple-element.3) | copy-start | bytes 196612
  231.2 15.8 %copy-start.8 = (f32[2048]{0:T(1024)S(1)}, f32[2048]{0:T(1024)}, u32[]{:S(2)}) copy-start(f32[2048]{0:T(1024)} %param.26) | copy-start | bytes 24580
Sparse Core Ops, SparseCore 0:
  27.9 77.9 reduce-scatter.1
  163.9 14.3 all-reduce.3
  207.1 17.0 all-reduce.5
where the time goes:
time: 255 us; the launch traced here: 254 us
  waiting for transfers between devices  138 us (54%)
  blocking collectives  53.9 us (21%)
  matrix products  18.1 us (7%)
  starting transfers between devices  17.3 us (7%)
  between operations  14.1 us (6%)
  other arithmetic  11.2 us (4%)
    reduce_scatter x1, waiting for transfers between devices, on_device(): lax.psum_scatter(jnp.dot(features, joined, preferred_element_type=jnp.flo...  77.1 us
    all_gather x1, blocking collectives, on_device(): lax.all_gather(retained, 'ep', axis=0, tiled=True)  38.2 us
    psum x1, waiting for transfers between devices, on_device(): expert_sum = lax.psum(partial_out.astype(jnp.bfloat16), 'tp')  17.3 us
    all_to_all x1, blocking collectives, on_device(): lax.all_to_all(normed, 'ep', split_axis=1, concat_axis=0, tiled=True)  15.7 us
    psum x1, waiting for transfers between devices, on_device(): lax.psum(rounded(partial_mix).astype(jnp.bfloat16), 'tp')  14.5 us
    all_to_all x1, waiting for transfers between devices, on_device(): lax.all_to_all(expert_sum.reshape(sources, held_slots, -1), 'ep', split_a...  11.1 us
    all_to_all x1, waiting for transfers between devices, on_device(): lax.all_to_all(outgoing, 'ep', split_axis=0, concat_axis=0, tiled=True)  10.9 us
    all_to_all x1, waiting for transfers between devices, on_device(): lax.all_to_all(column_part, 'ep', split_axis=0, concat_axis=1, tiled=True)  7.44 us
  transfers between devices with their start and end apart: 6, of which 6 were waited for; matrix products, arithmetic and copies ran while one was open for 4% of the time, Pallas kernels for 0%

commit v1 on v0

v1 whole, which is shorter than its diff:
```python
import functools

import jax
import jax.numpy as jnp
from jax import lax
from jax.experimental import pallas as pl
from jax.experimental.pallas import tpu as pltpu
from jax.sharding import PartitionSpec as P

HEAD = 64
HEADS = 16
EPS = 1e-06
THETA = 10000.0
MESH = pl.DeviceIdType.MESH
F32 = jnp.float32
BF16 = jnp.bfloat16


def rotate(vectors, lengths):
    half_dim = vectors.shape[-1] // 2
    frequency = THETA ** (-jnp.arange(half_dim, dtype=jnp.float32) / half_dim)
    angles = lengths.astype(jnp.float32)[:, None] * frequency[None, :]
    cosine = jnp.cos(angles)[:, None, :]
    sine_part = jnp.sin(angles)[:, None, :]
    leading = vectors[..., :half_dim]
    trailing = vectors[..., half_dim:]
    return jnp.concatenate(
        [leading * cosine - trailing * sine_part, trailing * cosine + leading * sine_part], axis=-1
    )


def decay_table(head_count):
    head_order = jnp.arange(head_count, dtype=jnp.float32)
    return 1.0 - jnp.exp2(-5.0 - 7.0 * head_order / (head_count - 1))


def retain(queries, keys_new, values, out_gate, prior_state, lengths, decays):
    seq_count = queries.shape[0]
    head_count = decays.shape[0]
    layout = (seq_count, head_count, HEAD)
    rot_query = rotate(queries.astype(jnp.float32).reshape(layout), lengths)
    rot_key = rotate(keys_new.astype(jnp.float32).reshape(layout), lengths) * HEAD ** (-0.5)
    wide_values = values.astype(jnp.float32).reshape(layout)
    from_state = jnp.einsum(
        "shd,shde->she", rot_query, prior_state, precision=lax.Precision.HIGHEST
    )
    self_term = jnp.sum(rot_query * rot_key, axis=-1, keepdims=True)
    read_out = decays[None, :, None] * from_state + self_term * wide_values
    new_state = (
        decays[None, :, None, None] * prior_state
        + rot_key[..., :, None] * wide_values[..., None, :]
    )
    normed = read_out * lax.rsqrt(jnp.mean(read_out * read_out, axis=-1, keepdims=True) + EPS)
    gated_rows = normed.reshape(seq_count, head_count * HEAD) * jax.nn.silu(
        out_gate.astype(jnp.float32)
    )
    return (gated_rows.astype(jnp.bfloat16), new_state)


def norm_rows(wide, gain):
    return wide * lax.rsqrt(jnp.mean(wide * wide, axis=-1, keepdims=True) + EPS) * gain


class Place:
    def __init__(self, lows, highs):
        self.lows, self.highs = lows, highs
        self.count = lows * highs
        self.ep = lax.axis_index("ep")
        self.tp = lax.axis_index("tp")
        self.hi = self.ep // lows
        self.lo = lax.rem(self.ep, lows)

    def greet(self):
        barrier = pltpu.get_barrier_semaphore()
        total = 2 * self.count
        flat = self.ep * 2 + self.tp

        def body(i, carry):
            other = lax.rem(flat + i, total)
            pl.semaphore_signal(
                barrier, inc=1, device_id=(other // 2, lax.rem(other, 2)), device_id_type=MESH
            )
            return carry

        lax.fori_loop(1, total, body, 0)
        pl.semaphore_wait(barrier, total - 1)

    def all_peers(self, source_of, target, send, recv):
        def body(i, carry):
            other = lax.rem(self.ep + i, self.count)
            start(source_of(other), target, send, recv, (other, self.tp))
            return carry

        lax.fori_loop(1, self.count, body, 0)

    def low_peers(self, source_of, target, send, recv):
        def body(i, carry):
            other = lax.rem(self.lo + i, self.lows)
            start(source_of(other), target, send, recv, (self.hi * self.lows + other, self.tp))
            return carry

        lax.fori_loop(1, self.lows, body, 0)

    def high_peers(self, source_of, target, send, recv):
        def body(i, carry):
            other = lax.rem(self.hi + i, self.highs)
            start(source_of(other), target, send, recv, (other * self.lows + self.lo, self.tp))
            return carry

        lax.fori_loop(1, self.highs, body, 0)


def start(source, target, send, recv, device):
    pltpu.make_async_remote_copy(
        src_ref=source,
        dst_ref=target,
        send_sem=send,
        recv_sem=recv,
        device_id=device,
        device_id_type=MESH,
    ).start()


def drain(span, sem):
    pltpu.make_async_copy(span, span, sem).wait()


def gather_blocks(place, own, held, sems, first):
    lows, highs = place.lows, place.highs
    place.high_peers(
        lambda other: own, held.at[place.lo, place.hi], sems.at[first], sems.at[first + 1]
    )
    arrived = held.at[0, pl.ds(0, highs - 1)]
    drain(arrived, sems.at[first + 1])
    place.low_peers(
        lambda other: held.at[place.lo], held.at[place.lo], sems.at[first + 2], sems.at[first + 3]
    )
    drain(held.at[pl.ds(0, lows - 1)], sems.at[first + 3])
    drain(arrived, sems.at[first])
    drain(held.at[pl.ds(0, lows - 1)], sems.at[first + 2])


def scatter_sums(place, part, landed, halfway, last, sems, first):
    lows, highs = place.lows, place.highs
    place.low_peers(
        lambda other: part.at[other], landed.at[place.lo], sems.at[first], sems.at[first + 1]
    )
    landed[place.lo] = part[place.lo]
    drain(landed.at[pl.ds(0, lows - 1)], sems.at[first + 1])

    def fold(h, carry):
        total = landed[0, h].astype(F32)
        for l in range(1, lows):
            total = total + landed[l, h].astype(F32)
        halfway[h] = total.astype(BF16)
        return carry

    lax.fori_loop(0, highs, fold, 0)
    place.high_peers(
        lambda other: halfway.at[other],
        last.at[place.hi],
        sems.at[first + 2],
        sems.at[first + 3],
    )
    last[place.hi] = halfway[place.hi]
    drain(last.at[pl.ds(0, highs - 1)], sems.at[first + 3])
    total = last[0].astype(F32)
    for h in range(1, highs):
        total = total + last[h].astype(F32)
    drain(part.at[pl.ds(0, lows - 1)], sems.at[first])
    drain(halfway.at[pl.ds(0, highs - 1)], sems.at[first + 2])
    return total


def project_kernel(
    lows,
    highs,
    tokens,
    gain,
    weights_q,
    weights_k,
    weights_v,
    weights_g,
    gates,
    projected,
    gates_all,
    outgoing,
    features,
    part,
    landed,
    halfway,
    last,
    sems,
):
    place = Place(lows, highs)
    count = place.count
    width = weights_q.shape[0]
    cols = weights_q.shape[1]
    normed = norm_rows(tokens[...].astype(F32), gain[...]).astype(BF16)
    for j in range(count):
        outgoing[j] = normed[:, j * width : (j + 1) * width]
    place.greet()
    place.all_peers(
        lambda other: outgoing.at[other],
        features.at[place.lo, place.hi],
        sems.at[0],
        sems.at[1],
    )
    features[place.lo, place.hi] = outgoing[place.ep]
    place.all_peers(
        lambda other: gates, gates_all.at[place.lo * highs + place.hi], sems.at[2], sems.at[3]
    )
    gates_all[place.lo * highs + place.hi] = gates[...]
    drain(outgoing.at[pl.ds(0, count - 1)], sems.at[1])
    seqs = features.shape[2]

    def multiply(l, carry):
        rows = features[l].reshape(highs * seqs, width)
        for k, weight in enumerate((weights_q, weights_k, weights_v, weights_g)):
            piece = jnp.dot(rows, weight[...], preferred_element_type=F32).astype(BF16)
            part[l, :, :, k * cols : (k + 1) * cols] = piece.reshape(highs, seqs, cols)
        return carry

    lax.fori_loop(0, lows, multiply, 0)
    total = scatter_sums(place, part, landed, halfway, last, sems, 4)
    projected[...] = total.astype(BF16)
    drain(outgoing.at[pl.ds(0, count - 1)], sems.at[0])
    drain(gates_all.at[pl.ds(0, count - 1)], sems.at[3])
    drain(gates_all.at[pl.ds(0, count - 1)], sems.at[2])


def layer_kernel(
    lows,
    highs,
    retained,
    tokens,
    out_weight,
    post_gain,
    ffn_gain,
    out_gain,
    gates_all,
    expert_gate,
    expert_up,
    expert_down,
    shared_gate,
    shared_up,
    shared_down,
    result,
    eg,
    eu,
    ed,
    sg,
    su,
    sd,
    held,
    columns,
    mixed,
    normed_all,
    part,
    landed,
    halfway,
    last,
    pair,
    local_sems,
    sems,
):
    place = Place(lows, highs)
    count = place.count
    loads = [
        pltpu.make_async_copy(source, target, local_sems.at[i])
        for i, (source, target) in enumerate(
            (
                (shared_gate, sg),
                (shared_up, su),
                (shared_down, sd),
                (expert_gate.at[0], eg),
                (expert_up.at[0], eu),
                (expert_down.at[0], ed),
            )
        )
    ]
    for load in loads:
        load.start()
    place.greet()
    seqs = tokens.shape[0]
    width = out_weight.shape[1]
    held[place.lo, place.hi] = retained[...]
    gather_blocks(place, retained, held, sems, 0)

    def multiply(l, carry):
        rows = held[l].reshape(highs * seqs, held.shape[3])
        piece = jnp.dot(rows, out_weight[...], preferred_element_type=F32).astype(BF16)
        columns[pl.ds(l * highs, highs)] = piece.reshape(highs, seqs, width)
        return carry

    lax.fori_loop(0, lows, multiply, 0)
    own_slot = place.tp * count + place.ep

    def send_back(i, carry):
        other = lax.rem(place.ep * 2 + place.tp + i, 2 * count)
        chip = other // 2
        slot = lax.rem(chip, lows) * highs + chip // lows
        start(
            columns.at[slot],
            mixed.at[own_slot],
            sems.at[4],
            sems.at[5],
            (chip, lax.rem(other, 2)),
        )
        return carry

    lax.fori_loop(1, 2 * count, send_back, 0)
    mixed[own_slot] = columns[place.lo * highs + place.hi]
    drain(mixed.at[pl.ds(0, 2 * count - 1)], sems.at[5])
    mixed_sum = jnp.concatenate(
        [(mixed[e].astype(F32) + mixed[count + e].astype(F32)) for e in range(count)], axis=1
    )
    mixed_sum = mixed_sum.astype(BF16).astype(F32)
    middle = tokens[...].astype(F32) + norm_rows(mixed_sum, post_gain[...])
    middle = middle.astype(BF16).astype(F32)
    moe_in = norm_rows(middle, ffn_gain[...]).astype(BF16)
    normed_all[place.lo, place.hi] = moe_in
    place_own = normed_all.at[place.lo, place.hi]

    gather_blocks(place, place_own, normed_all, sems, 6)
    for load in loads:
        load.wait()
    shared_hidden = (
        jax.nn.silu(jnp.dot(moe_in, sg[...], preferred_element_type=F32))
        * jnp.dot(moe_in, su[...], preferred_element_type=F32)
    ).astype(BF16)
    shared_part = jnp.dot(shared_hidden, sd[...], preferred_element_type=F32)

    chunk = max(1, min(lows, 256 // (highs * seqs)))
    chunk_rows = chunk * highs * seqs
    model = tokens.shape[1]

    def expert(i, carry):
        rows = normed_all[pl.ds(i * chunk, chunk)].reshape(chunk_rows, model)
        gate_rows = gates_all[pl.ds(i * chunk * highs, chunk * highs)].reshape(chunk_rows, count)
        lane = lax.broadcasted_iota(jnp.int32, (chunk_rows, count), 1)
        weight = jnp.sum(jnp.where(lane == place.ep, gate_rows, 0.0), axis=1, keepdims=True)
        hidden = (
            jax.nn.silu(jnp.dot(rows, eg[...], preferred_element_type=F32))
            * jnp.dot(rows, eu[...], preferred_element_type=F32)
        ).astype(BF16)
        piece = jnp.dot(hidden, ed[...], preferred_element_type=F32) * weight
        part[pl.ds(i * chunk, chunk)] = piece.astype(BF16).reshape(chunk, highs, seqs, model)
        return carry

    lax.fori_loop(0, lows // chunk, expert, 0)
    total = scatter_sums(place, part, landed, halfway, last, sems, 10)
    pair[0] = (total + shared_part).astype(BF16)
    start(pair.at[0], pair.at[1], sems.at[14], sems.at[15], (place.ep, 1 - place.tp))
    drain(pair.at[1], sems.at[15])
    mixture = pair[0].astype(F32) + pair[1].astype(F32)
    result[...] = (middle + norm_rows(mixture, out_gain[...])).astype(BF16)
    drain(mixed.at[pl.ds(0, 2 * count - 1)], sems.at[4])
    drain(pair.at[0], sems.at[14])


VM = pl.BlockSpec(memory_space=pltpu.VMEM)
FAR = pl.BlockSpec(memory_space=pl.ANY)


def on_device(
    lows,
    highs,
    tokens,
    lengths,
    prior_state,
    mix_gain,
    post_gain,
    ffn_gain,
    out_gain,
    query_weight,
    key_weight,
    value_weight,
    gate_weight,
    out_weight,
    routes,
    route_gates,
    expert_gate,
    expert_up,
    expert_down,
    shared_gate,
    shared_up,
    shared_down,
):
    count = lows * highs
    seqs, model = tokens.shape
    width, local_cols = query_weight.shape
    four = 4 * local_cols
    experts = jnp.arange(count, dtype=jnp.int32)
    gates = jnp.sum(
        jnp.where(
            routes[:, :, None] == experts[None, None, :], route_gates[:, :, None], jnp.float32(0)
        ),
        axis=1,
    )
    projected, gates_all = pl.pallas_call(
        functools.partial(project_kernel, lows, highs),
        out_shape=(
            jax.ShapeDtypeStruct((seqs, four), BF16),
            jax.ShapeDtypeStruct((count, seqs, count), F32),
        ),
        in_specs=[VM] * 7,
        out_specs=(VM, VM),
        scratch_shapes=[
            pltpu.VMEM((count, seqs, width), BF16),
            pltpu.VMEM((lows, highs, seqs, width), BF16),
            pltpu.VMEM((lows, highs, seqs, four), BF16),
            pltpu.VMEM((lows, highs, seqs, four), BF16),
            pltpu.VMEM((highs, seqs, four), BF16),
            pltpu.VMEM((highs, seqs, four), BF16),
            pltpu.SemaphoreType.DMA((8,)),
        ],
        compiler_params=pltpu.CompilerParams(collective_id=0, has_side_effects=True),
        name="project",
    )(
        tokens,
        mix_gain.reshape(1, -1),
        query_weight,
        key_weight,
        value_weight,
        gate_weight,
        gates,
    )
    queries, keys_new, values, out_gate = tuple(
        projected[:, role * local_cols : (role + 1) * local_cols] for role in range(4)
    )
    heads_here = local_cols // HEAD
    decays = lax.dynamic_slice_in_dim(
        decay_table(HEADS), lax.axis_index("tp") * heads_here, heads_here, 0
    )
    retained, new_state = retain(queries, keys_new, values, out_gate, prior_state, lengths, decays)
    hidden_cols = expert_gate.shape[2]
    shared_cols = shared_gate.shape[1]
    result = pl.pallas_call(
        functools.partial(layer_kernel, lows, highs),
        out_shape=jax.ShapeDtypeStruct((seqs, model), BF16),
        in_specs=[VM] * 7 + [FAR] * 6,
        out_specs=VM,
        scratch_shapes=[
            pltpu.VMEM((model, hidden_cols), BF16),
            pltpu.VMEM((model, hidden_cols), BF16),
            pltpu.VMEM((hidden_cols, model), BF16),
            pltpu.VMEM((model, shared_cols), BF16),
            pltpu.VMEM((model, shared_cols), BF16),
            pltpu.VMEM((shared_cols, model), BF16),
            pltpu.VMEM((lows, highs, seqs, local_cols), BF16),
            pltpu.VMEM((count, seqs, width), BF16),
            pltpu.VMEM((2 * count, seqs, width), BF16),
            pltpu.VMEM((lows, highs, seqs, model), BF16),
            pltpu.VMEM((lows, highs, seqs, model), BF16),
            pltpu.VMEM((lows, highs, seqs, model), BF16),
            pltpu.VMEM((highs, seqs, model), BF16),
            pltpu.VMEM((highs, seqs, model), BF16),
            pltpu.VMEM((2, seqs, model), BF16),
            pltpu.SemaphoreType.DMA((6,)),
            pltpu.SemaphoreType.DMA((16,)),
        ],
        compiler_params=pltpu.CompilerParams(collective_id=1, has_side_effects=True),
        name="layer",
    )(
        retained,
        tokens,
        out_weight,
        post_gain.reshape(1, -1),
        ffn_gain.reshape(1, -1),
        out_gain.reshape(1, -1),
        gates_all,
        expert_gate,
        expert_up,
        expert_down,
        shared_gate,
        shared_up,
        shared_down,
    )
    return (result, new_state)


def solution(mesh):
    count = mesh.shape["ep"]
    lows = 1
    while lows * lows < count:
        lows *= 2
    highs = count // lows
    return jax.shard_map(
        functools.partial(on_device, lows, highs),
        mesh=mesh,
        in_specs=(
            P("ep", None),
            P("ep"),
            P("ep", "tp", None, None),
            P(),
            P(),
            P(),
            P(),
            P("ep", "tp"),
            P("ep", "tp"),
            P("ep", "tp"),
            P("ep", "tp"),
            P("tp", "ep"),
            P("ep", None),
            P("ep", None),
            P("ep", None, "tp"),
            P("ep", None, "tp"),
            P("ep", "tp", None),
            P(None, "tp"),
            P(None, "tp"),
            P("tp", None),
        ),
        out_specs=(P("ep", None), P("ep", "tp", None, None)),
        check_vma=False,
    )
```

time: 255 us -> 109 us (0.43)
  waiting for transfers between devices: 138 us -> 0 us
  Pallas kernels: 0 us -> 92.6 us
  blocking collectives: 53.9 us -> 0 us
  starting transfers between devices: 17.3 us -> 0 us
  between operations: 14.1 us -> 0.71 us
  matrix products: 18.1 us -> 5.29 us
    pallas_call x0 -> x2, Pallas kernels: none -> 92.6 us  [the longest x1 59.8 us: on_device(): pl.pallas_call(functools.partial(layer_kernel, lows, highs), out_shape=ja...]
    reduce_scatter x1 -> x0, waiting for transfers between devices: 77.1 us -> none  [on_device(): lax.psum_scatter(jnp.dot(features, joined, preferred_element_type=jnp.flo...]
    all_gather x1 -> x0, blocking collectives: 38.2 us -> none  [on_device(): lax.all_gather(retained, 'ep', axis=0, tiled=True)]
    psum x2 -> x0, waiting for transfers between devices: 31.7 us -> none  [the longest x1 17.3 us: on_device(): expert_sum = lax.psum(partial_out.astype(jnp.bfloat16), 'tp')]
    all_to_all x3 -> x0, waiting for transfers between devices: 29.5 us -> none  [the longest x1 11.1 us: on_device(): lax.all_to_all(expert_sum.reshape(sources, held_slots, -1), 'ep', split_a...]
    all_to_all x3 -> x0, starting transfers between devices: 17.2 us -> none  [the longest x1 6.84 us: on_device(): lax.all_to_all(outgoing, 'ep', split_axis=0, concat_axis=0, tiled=True)]
    all_to_all x1 -> x0, blocking collectives: 15.7 us -> none  [on_device(): lax.all_to_all(normed, 'ep', split_axis=1, concat_axis=0, tiled=True)]
    dot_general x8 -> x0, matrix products: 12.8 us -> none  [the longest x1 2.97 us: on_device(): jnp.dot(shared_hidden, shared_down, preferred_element_type=jnp.float32)]
  transfers between devices with their start and end apart: 6 -> 0, of which waited for: 6 -> 0; matrix products, arithmetic and copies ran while one was open for 4% -> 0% of each run, Pallas kernels for 0% -> 0%
where the time goes in v1:
time: 109 us
  Pallas kernels  92.6 us (85%)
  other arithmetic  9.11 us (8%)
  matrix products  5.29 us (5%)
    pallas_call x1, Pallas kernels, on_device(): pl.pallas_call(functools.partial(layer_kernel, lows, highs), out_shape=ja...  59.8 us
    pallas_call x1, Pallas kernels, on_device(): pl.pallas_call(functools.partial(project_kernel, lows, highs), out_shape=...  32.8 us
    dot_general x1, matrix products, retain(): jnp.einsum('shd,shde->she', rot_query, prior_state, precision=lax.Precisi...  5.29 us
    add x1, other arithmetic, retain(): decays[None, :, None, None] * prior_state  4.3 us

profile of v1, /device:TPU:0, one launch (start us, length us, event | category | flops | bytes accessed | tf_op | source)
XLA Modules:
  0.0 108.8 jit_solution(14240048504693890556)
XLA Ops:
  0.6 0.7 convert_element_type.6
  1.3 0.1 dynamic_slice.3
  1.4 1.4 %select_reduce_fusion.gates = f32[16,16]{1,0:T(8,128)} fusion(f32[16,6]{0,1:T(8,128)} %param.33, s32[16,6]{0,1:T(8,128)} %param.32), kind=kLoop, calls=%fused_computation.11 | loop fusion | flops 4352 | bytes 1792 | tf_op jit(solution)/shard_map/reduce_sum | solution.py:395
  2.8 0.1 multiply_cosine_fusion
  2.9 32.8 %project.1 = (bf16[16,2048]{1,0:T(8,128)(2,1)}, f32[16,16,16]{2,1,0:T(8,128)}) custom-call(bf16[16,2048]{1,0:T(8,128)(2,1)} %tokens.3, f32[1,2048]{1,0:T(1,128)} %bitcast.13, bf16[128,512]{1,0:T(8,128)(2,1)} %weights_q.1, bf16[128,512]{1,0:T(8,128)(2,1)} %weights_k.1, bf16[128,512]{1,0:T(8,128)(2,1)} %weights_v.1, bf16[128,512]{1,0:T(8,128)(2,1)} %weights_g.1, ...), custom_call_target="tpu_custom_call" | custom-call | tf_op jit(solution)/shard_map/project/pallas_call | solution.py:401
  35.7 0.8 slice_convert_fusion.1
  36.5 0.1 reshape.131
  36.6 0.1 reshape.133
  36.7 0.1 reshape.129
  36.7 0.1 multiply_subtract_fusion
  36.8 0.1 pad_maximum_fusion
  37.0 5.3 %fusion.9 = f32[16,8,1,64]{3,2,1,0:T(1,128)S(1)} fusion(f32[16,8,64,1]{2,3,1,0:T(1,128)S(1)} %bitcast.11, f32[16,8,64,64]{3,2,1,0:T(8,128)} %param.22), kind=kOutput, calls=%fused_computation.31 | convolution fusion | flops 6291456 | bytes 2162688 | tf_op jit(solution)/shard_map/shd,shde->she/dot_general | solution.py:44
  42.3 0.2 multiply_reduce_fusion
  42.5 0.1 broadcast_multiply_fusion
  42.6 0.1 reshape.124
  42.6 1.3 %fusion.7.retained = bf16[16,512]{1,0:T(8,128)(2,1)} fusion(f32[16,512]{1,0:T(8,128)S(1)} %reshape.124, bf16[16,2048]{1,0:T(8,128)(2,1)} %get-tuple-element.4), kind=kLoop, calls=%fused_computation.20 | loop fusion | flops 57344 | bytes 65536 | tf_op jit(solution)/shard_map/convert_element_type | solution.py:57
  44.0 59.8 %layer.1 = bf16[16,2048]{1,0:T(8,128)(2,1)} custom-call(bf16[16,512]{1,0:T(8,128)(2,1)} %fusion.7.retained, bf16[16,2048]{1,0:T(8,128)(2,1)} %tokens.3, bf16[512,128]{1,0:T(8,128)(2,1)} %out_weight.1, f32[1,2048]{1,0:T(1,128)} %bitcast.14, f32[1,2048]{1,0:T(1,128)} %bitcast.15, f32[1,2048]{1,0:T(1,128)} %bitcast.16, ...), custom_call_target="tpu_custom_call" | custom-call | tf_op jit(solution)/shard_map/layer/pallas_call | solution.py:439
  103.8 0.0 copy-start
  103.8 4.3 %multiply_add_fusion = f32[16,8,64,64]{3,2,1,0:T(8,128)} fusion(f32[16,8,64,64]{3,2,1,0:T(8,128)} %param.22, f32[16,8,64]{2,1,0:T(8,128)S(1)} %reshape.133, f32[16,8,64]{2,1,0:T(8,128)S(1)} %get-tuple-element.20, f32[8]{0:T(128)S(1)} %dynamic_slice.3), kind=kLoop, calls=%fused_computation.1 | loop fusion | flops 1572864 | bytes 4259872 | tf_op jit(solution)/shard_map/add | solution.py:50
  108.1 0.0 copy-done
  108.1 0.6 copy.27
  (3 shorter events, 0.0 us)
Async XLA Ops:
  103.8 4.3 %copy-start = (bf16[16,2048]{1,0:T(8,128)(2,1)S(1)}, bf16[16,2048]{1,0:T(8,128)(2,1)}, u32[]{:S(2)}) copy-start(bf16[16,2048]{1,0:T(8,128)(2,1)} %layer.1) | copy-start | bytes 196612

commit v2 on v1

--- a/solution.py
+++ b/solution.py
@@ -125,51 +125,68 @@
     pltpu.make_async_copy(span, span, sem).wait()
 
 
-def gather_blocks(place, own, held, sems, first):
+def gather_blocks(place, held, send, near, far, during=None, arrived=None):
     lows, highs = place.lows, place.highs
-    place.high_peers(
-        lambda other: own, held.at[place.lo, place.hi], sems.at[first], sems.at[first + 1]
-    )
-    arrived = held.at[0, pl.ds(0, highs - 1)]
-    drain(arrived, sems.at[first + 1])
-    place.low_peers(
-        lambda other: held.at[place.lo], held.at[place.lo], sems.at[first + 2], sems.at[first + 3]
-    )
-    drain(held.at[pl.ds(0, lows - 1)], sems.at[first + 3])
-    drain(arrived, sems.at[first])
-    drain(held.at[pl.ds(0, lows - 1)], sems.at[first + 2])
-
-
-def scatter_sums(place, part, landed, halfway, last, sems, first):
+    own = held.at[place.lo, place.hi]
+    place.high_peers(lambda other: own, own, send.at[0], far.at[place.hi])
+    place.low_peers(lambda other: own, own, send.at[1], near.at[place.hi])
+    if during is not None:
+        during()
+    for i in range(1, highs):
+        h = lax.rem(place.hi + highs - i, highs)
+        block = held.at[place.lo, h]
+        drain(block, far.at[h])
+        place.low_peers(lambda other: block, block, send.at[1], near.at[h])
+    for i in range(highs):
+        h = lax.rem(place.hi + highs - i, highs)
+        drain(held.at[pl.ds(0, lows - 1), h], near.at[h])
+        if arrived is not None:
+            arrived(h)
+
+    def finish():
+        drain(held.at[0, pl.ds(0, highs - 1)], send.at[0])
+        drain(held.at[pl.ds(0, lows - 1)], send.at[1])
+
+    return finish
+
+
+def scatter_sums(place, fill, part, landed, halfway, last, send, near, far):
     lows, highs = place.lows, place.highs
-    place.low_peers(
-        lambda other: part.at[other], landed.at[place.lo], sems.at[first], sems.at[first + 1]
-    )
-    landed[place.lo] = part[place.lo]
-    drain(landed.at[pl.ds(0, lows - 1)], sems.at[first + 1])
-
-    def fold(h, carry):
-        total = landed[0, h].astype(F32)
-        for l in range(1, lows):
-            total = total + landed[l, h].astype(F32)
-        halfway[h] = total.astype(BF16)
-        return carry
-
-    lax.fori_loop(0, highs, fold, 0)
-    place.high_peers(
-        lambda other: halfway.at[other],
-        last.at[place.hi],
-        sems.at[first + 2],
-        sems.at[first + 3],
-    )
-    last[place.hi] = halfway[place.hi]
-    drain(last.at[pl.ds(0, highs - 1)], sems.at[first + 3])
-    total = last[0].astype(F32)
-    for h in range(1, highs):
-        total = total + last[h].astype(F32)
-    drain(part.at[pl.ds(0, lows - 1)], sems.at[first])
-    drain(halfway.at[pl.ds(0, highs - 1)], sems.at[first + 2])
-    return total
+    chunks = part.shape[0]
+    for c in range(chunks):
+        fill(c)
+        place.low_peers(
+            lambda other: part.at[c, other], landed.at[c, place.lo], send.at[0], near.at[c]
+        )
+        landed[c, place.lo] = part[c, place.lo]
+    for c in range(chunks):
+        drain(landed.at[c, pl.ds(0, lows - 1)], near.at[c])
+
+        def fold(h, carry):
+            total = landed[c, 0, h].astype(F32)
+            for l in range(1, lows):
+                total = total + landed[c, l, h].astype(F32)
+            halfway[c, h] = total.astype(BF16)
+            return carry
+
+        lax.fori_loop(0, highs, fold, 0)
+        place.high_peers(
+            lambda other: halfway.at[c, other], last.at[c, place.hi], send.at[1], far.at[c]
+        )
+        last[c, place.hi] = halfway[c, place.hi]
+    sums = []
+    for c in range(chunks):
+        drain(last.at[c, pl.ds(0, highs - 1)], far.at[c])
+        total = last[c, 0].astype(F32)
+        for h in range(1, highs):
+            total = total + last[c, h].astype(F32)
+        sums.append(total)
+
+    def finish():
+        drain(part.at[:, pl.ds(0, lows - 1)], send.at[0])
+        drain(halfway.at[:, pl.ds(0, highs - 1)], send.at[1])
+
+    return sums, finish
 
 
 def project_kernel(
@@ -191,6 +208,9 @@
     halfway,
     last,
     sems,
+    send,
+    near,
+    far,
 ):
     place = Place(lows, highs)
     count = place.count
@@ -213,17 +233,21 @@
     gates_all[place.lo * highs + place.hi] = gates[...]
     drain(outgoing.at[pl.ds(0, count - 1)], sems.at[1])
     seqs = features.shape[2]
-
-    def multiply(l, carry):
-        rows = features[l].reshape(highs * seqs, width)
-        for k, weight in enumerate((weights_q, weights_k, weights_v, weights_g)):
-            piece = jnp.dot(rows, weight[...], preferred_element_type=F32).astype(BF16)
-            part[l, :, :, k * cols : (k + 1) * cols] = piece.reshape(highs, seqs, cols)
-        return carry
-
-    lax.fori_loop(0, lows, multiply, 0)
-    total = scatter_sums(place, part, landed, halfway, last, sems, 4)
-    projected[...] = total.astype(BF16)
+    weights = (weights_q, weights_k, weights_v, weights_g)
+
+    def fill(c):
+        def multiply(l, carry):
+            rows = features[l].reshape(highs * seqs, width)
+            piece = jnp.dot(rows, weights[c][...], preferred_element_type=F32).astype(BF16)
+            part[c, l] = piece.reshape(highs, seqs, cols)
+            return carry
+
+        lax.fori_loop(0, lows, multiply, 0)
+
+    sums, finish = scatter_sums(place, fill, part, landed, halfway, last, send, near, far)
+    for c in range(4):
+        projected[:, c * cols : (c + 1) * cols] = sums[c].astype(BF16)
+    finish()
     drain(outgoing.at[pl.ds(0, count - 1)], sems.at[0])
     drain(gates_all.at[pl.ds(0, count - 1)], sems.at[3])
     drain(gates_all.at[pl.ds(0, count - 1)], sems.at[2])
@@ -256,6 +280,12 @@
     columns,
     mixed,
     normed_all,
+    gate_sum,
+    up_sum,
+    hidden,
+    shared_pair,
+    give,
+    theirs,
     part,
     landed,
     halfway,
@@ -263,9 +293,21 @@
     pair,
     local_sems,
     sems,
+    held_send,
+    held_near,
+    held_far,
+    all_send,
+    all_near,
+    all_far,
+    all_twin,
+    sum_send,
+    sum_near,
+    sum_far,
+    sum_twin,
 ):
     place = Place(lows, highs)
     count = place.count
+    twin = (place.ep, 1 - place.tp)
     loads = [
         pltpu.make_async_copy(source, target, local_sems.at[i])
         for i, (source, target) in enumerate(
@@ -282,10 +324,11 @@
     for load in loads:
         load.start()
     place.greet()
-    seqs = tokens.shape[0]
+    seqs, model = tokens.shape
+    half = model // 2
     width = out_weight.shape[1]
     held[place.lo, place.hi] = retained[...]
-    gather_blocks(place, retained, held, sems, 0)
+    finish_held = gather_blocks(place, held, held_send, held_near, held_far)
 
     def multiply(l, carry):
         rows = held[l].reshape(highs * seqs, held.shape[3])
@@ -303,15 +346,17 @@
         start(
             columns.at[slot],
             mixed.at[own_slot],
-            sems.at[4],
-            sems.at[5],
+            sems.at[0],
+            sems.at[1],
             (chip, lax.rem(other, 2)),
         )
         return carry
 
     lax.fori_loop(1, 2 * count, send_back, 0)
     mixed[own_slot] = columns[place.lo * highs + place.hi]
-    drain(mixed.at[pl.ds(0, 2 * count - 1)], sems.at[5])
+    for load in loads:
+        load.wait()
+    drain(mixed.at[pl.ds(0, 2 * count - 1)], sems.at[1])
     mixed_sum = jnp.concatenate(
         [(mixed[e].astype(F32) + mixed[count + e].astype(F32)) for e in range(count)], axis=1
     )
@@ -319,44 +364,104 @@
     middle = tokens[...].astype(F32) + norm_rows(mixed_sum, post_gain[...])
     middle = middle.astype(BF16).astype(F32)
     moe_in = norm_rows(middle, ffn_gain[...]).astype(BF16)
-    normed_all[place.lo, place.hi] = moe_in
-    place_own = normed_all.at[place.lo, place.hi]
-
-    gather_blocks(place, place_own, normed_all, sems, 6)
-    for load in loads:
-        load.wait()
-    shared_hidden = (
-        jax.nn.silu(jnp.dot(moe_in, sg[...], preferred_element_type=F32))
-        * jnp.dot(moe_in, su[...], preferred_element_type=F32)
-    ).astype(BF16)
-    shared_part = jnp.dot(shared_hidden, sd[...], preferred_element_type=F32)
+    own_half = jnp.where(place.tp == 0, moe_in[:, :half], moe_in[:, half:])
+    normed_all[place.tp, place.lo, place.hi] = own_half
+    mine = normed_all.at[place.tp]
+
+    def shared():
+        shared_hidden = (
+            jax.nn.silu(jnp.dot(moe_in, sg[...], preferred_element_type=F32))
+            * jnp.dot(moe_in, su[...], preferred_element_type=F32)
+        ).astype(BF16)
+        shared_part = jnp.dot(shared_hidden, sd[...], preferred_element_type=F32).astype(BF16)
+        for t in range(2):
+            shared_pair[t] = shared_part[:, t * half : (t + 1) * half]
+        start(shared_pair.at[1 - place.tp], shared_pair.at[2], sems.at[2], sems.at[3], twin)
+
+    def hand_over(h):
+        start(
+            mine.at[:, h],
+            normed_all.at[place.tp, :, h],
+            sems.at[4],
+            all_twin,
+            twin,
+        )
+
+    finish_all = gather_blocks(place, mine, all_send, all_near, all_far, shared, hand_over)
 
     chunk = max(1, min(lows, 256 // (highs * seqs)))
     chunk_rows = chunk * highs * seqs
-    model = tokens.shape[1]
-
-    def expert(i, carry):
-        rows = normed_all[pl.ds(i * chunk, chunk)].reshape(chunk_rows, model)
+    steps = lows // chunk
+    own_rows = pl.ds(pl.multiple_of(place.tp * half, half), half)
+    other_rows = pl.ds(pl.multiple_of((1 - place.tp) * half, half), half)
+
+    def near_half(i, carry):
+        rows = normed_all[place.tp, pl.ds(i * chunk, chunk)].reshape(chunk_rows, half)
+        gate_sum[i] = jnp.dot(rows, eg[own_rows, :], preferred_element_type=F32)
+        up_sum[i] = jnp.dot(rows, eu[own_rows, :], preferred_element_type=F32)
+        return carry
+
+    lax.fori_loop(0, steps, near_half, 0)
+    drain(normed_all.at[1 - place.tp], all_twin)
+
+    def far_half(i, carry):
+        rows = normed_all[1 - place.tp, pl.ds(i * chunk, chunk)].reshape(chunk_rows, half)
+        gate_cols = gate_sum[i] + jnp.dot(rows, eg[other_rows, :], preferred_element_type=F32)
+        up_cols = up_sum[i] + jnp.dot(rows, eu[other_rows, :], preferred_element_type=F32)
+        hidden[i] = (jax.nn.silu(gate_cols) * up_cols).astype(BF16)
+        return carry
+
+    lax.fori_loop(0, steps, far_half, 0)
+    cols = part.shape[4]
+
+    def down(i, first):
         gate_rows = gates_all[pl.ds(i * chunk * highs, chunk * highs)].reshape(chunk_rows, count)
         lane = lax.broadcasted_iota(jnp.int32, (chunk_rows, count), 1)
         weight = jnp.sum(jnp.where(lane == place.ep, gate_rows, 0.0), axis=1, keepdims=True)
-        hidden = (
-            jax.nn.silu(jnp.dot(rows, eg[...], preferred_element_type=F32))
-            * jnp.dot(rows, eu[...], preferred_element_type=F32)
-        ).astype(BF16)
-        piece = jnp.dot(hidden, ed[...], preferred_element_type=F32) * weight
-        part[pl.ds(i * chunk, chunk)] = piece.astype(BF16).reshape(chunk, highs, seqs, model)
-        return carry
-
-    lax.fori_loop(0, lows // chunk, expert, 0)
-    total = scatter_sums(place, part, landed, halfway, last, sems, 10)
-    pair[0] = (total + shared_part).astype(BF16)
-    start(pair.at[0], pair.at[1], sems.at[14], sems.at[15], (place.ep, 1 - place.tp))
-    drain(pair.at[1], sems.at[15])
-    mixture = pair[0].astype(F32) + pair[1].astype(F32)
+        span = pl.ds(pl.multiple_of(first, cols), cols)
+        return jnp.dot(hidden[i], ed[:, span], preferred_element_type=F32) * weight
+
+    for c in range(part.shape[0]):
+
+        def outward(i, carry):
+            piece = down(i, (1 - place.tp) * half + c * cols).astype(BF16)
+            give[c, pl.ds(i * chunk, chunk)] = piece.reshape(chunk, highs, seqs, cols)
+            return carry
+
+        lax.fori_loop(0, steps, outward, 0)
+        start(give.at[c], theirs.at[c], sems.at[5], sum_twin.at[c], twin)
+
+    def fill(c):
+        drain(theirs.at[c], sum_twin.at[c])
+
+        def inward(i, carry):
+            piece = down(i, place.tp * half + c * cols)
+            other = theirs[c, pl.ds(i * chunk, chunk)].reshape(chunk_rows, cols).astype(F32)
+            piece = (piece + other).astype(BF16)
+            part[c, pl.ds(i * chunk, chunk)] = piece.reshape(chunk, highs, seqs, cols)
+            return carry
+
+        lax.fori_loop(0, steps, inward, 0)
+
+    sums, finish_sums = scatter_sums(
+        place, fill, part, landed, halfway, last, sum_send, sum_near, sum_far
+    )
+    drain(shared_pair.at[2], sems.at[3])
+    pair[place.tp] = jnp.concatenate(sums, axis=1) + (
+        shared_pair[place.tp].astype(F32) + shared_pair[2].astype(F32)
+    )
+    start(pair.at[place.tp], pair.at[place.tp], sems.at[6], sems.at[7], twin)
+    drain(pair.at[1 - place.tp], sems.at[7])
+    mixture = jnp.concatenate([pair[0], pair[1]], axis=1)
     result[...] = (middle + norm_rows(mixture, out_gain[...])).astype(BF16)
-    drain(mixed.at[pl.ds(0, 2 * count - 1)], sems.at[4])
-    drain(pair.at[0], sems.at[14])
+    finish_held()
+    finish_all()
+    finish_sums()
+    drain(mixed.at[pl.ds(0, 2 * count - 1)], sems.at[0])
+    drain(shared_pair.at[2], sems.at[2])
+    drain(mine, sems.at[4])
+    drain(give, sems.at[5])
+    drain(pair.at[0], sems.at[6])
 
 
 VM = pl.BlockSpec(memory_space=pltpu.VMEM)
@@ -409,11 +514,14 @@
         scratch_shapes=[
             pltpu.VMEM((count, seqs, width), BF16),
             pltpu.VMEM((lows, highs, seqs, width), BF16),
-            pltpu.VMEM((lows, highs, seqs, four), BF16),
-            pltpu.VMEM((lows, highs, seqs, four), BF16),
-            pltpu.VMEM((highs, seqs, four), BF16),
-            pltpu.VMEM((highs, seqs, four), BF16),
-            pltpu.SemaphoreType.DMA((8,)),
+            pltpu.VMEM((4, lows, highs, seqs, local_cols), BF16),
+            pltpu.VMEM((4, lows, highs, seqs, local_cols), BF16),
+            pltpu.VMEM((4, highs, seqs, local_cols), BF16),
+            pltpu.VMEM((4, highs, seqs, local_cols), BF16),
+            pltpu.SemaphoreType.DMA((4,)),
+            pltpu.SemaphoreType.DMA((2,)),
+            pltpu.SemaphoreType.DMA((4,)),
+            pltpu.SemaphoreType.DMA((4,)),
         ],
         compiler_params=pltpu.CompilerParams(collective_id=0, has_side_effects=True),
         name="project",
@@ -436,6 +544,9 @@
     retained, new_state = retain(queries, keys_new, values, out_gate, prior_state, lengths, decays)
     hidden_cols = expert_gate.shape[2]
     shared_cols = shared_gate.shape[1]
+    half = model // 2
+    chunks = 4
+    steps = lows // max(1, min(lows, 256 // (highs * seqs)))
     result = pl.pallas_call(
         functools.partial(layer_kernel, lows, highs),
         out_shape=jax.ShapeDtypeStruct((seqs, model), BF16),
@@ -451,14 +562,31 @@
             pltpu.VMEM((lows, highs, seqs, local_cols), BF16),
             pltpu.VMEM((count, seqs, width), BF16),
             pltpu.VMEM((2 * count, seqs, width), BF16),
-            pltpu.VMEM((lows, highs, seqs, model), BF16),
-            pltpu.VMEM((lows, highs, seqs, model), BF16),
-            pltpu.VMEM((lows, highs, seqs, model), BF16),
-            pltpu.VMEM((highs, seqs, model), BF16),
-            pltpu.VMEM((highs, seqs, model), BF16),
-            pltpu.VMEM((2, seqs, model), BF16),
+            pltpu.VMEM((2, lows, highs, seqs, half), BF16),
+            pltpu.VMEM((steps, count * seqs // steps, hidden_cols), F32),
+            pltpu.VMEM((steps, count * seqs // steps, hidden_cols), F32),
+            pltpu.VMEM((steps, count * seqs // steps, hidden_cols), BF16),
+            pltpu.VMEM((3, seqs, half), BF16),
+            pltpu.VMEM((chunks, lows, highs, seqs, half // chunks), BF16),
+            pltpu.VMEM((chunks, lows, highs, seqs, half // chunks), BF16),
+            pltpu.VMEM((chunks, lows, highs, seqs, half // chunks), BF16),
+            pltpu.VMEM((chunks, lows, highs, seqs, half // chunks), BF16),
+            pltpu.VMEM((chunks, highs, seqs, half // chunks), BF16),
+            pltpu.VMEM((chunks, highs, seqs, half // chunks), BF16),
+            pltpu.VMEM((2, seqs, half), F32),
             pltpu.SemaphoreType.DMA((6,)),
-            pltpu.SemaphoreType.DMA((16,)),
+            pltpu.SemaphoreType.DMA((8,)),
+            pltpu.SemaphoreType.DMA((2,)),
+            pltpu.SemaphoreType.DMA((highs,)),
+            pltpu.SemaphoreType.DMA((highs,)),
+            pltpu.SemaphoreType.DMA((2,)),
+            pltpu.SemaphoreType.DMA((highs,)),
+            pltpu.SemaphoreType.DMA((highs,)),
+            pltpu.SemaphoreType.DMA,
+            pltpu.SemaphoreType.DMA((2,)),
+            pltpu.SemaphoreType.DMA((chunks,)),
+            pltpu.SemaphoreType.DMA((chunks,)),
+            pltpu.SemaphoreType.DMA((chunks,)),
         ],
         compiler_params=pltpu.CompilerParams(collective_id=1, has_side_effects=True),
         name="layer",

time: 109 us -> 89.8 us (0.82)
  Pallas kernels: 92.6 us -> 73.4 us
    pallas_call x1, Pallas kernels: 59.8 us -> 42.9 us  [on_device(): pl.pallas_call(functools.partial(layer_kernel, lows, highs), out_shape=ja...]
    pallas_call x1, Pallas kernels: 32.8 us -> 30.5 us  [on_device(): pl.pallas_call(functools.partial(project_kernel, lows, highs), out_shape=...]
where the time goes in v2:
time: 89.8 us; the launch traced here: 89.5 us
  Pallas kernels  73.4 us (82%)
  other arithmetic  9.11 us (10%)
  matrix products  5.29 us (6%)
  local copies, waits for them, and re-layouts  1.02 us (1%)
    pallas_call x1, Pallas kernels, on_device(): pl.pallas_call(functools.partial(layer_kernel, lows, highs), out_shape=ja...  42.9 us
    pallas_call x1, Pallas kernels, on_device(): pl.pallas_call(functools.partial(project_kernel, lows, highs), out_shape=...  30.5 us
    dot_general x1, matrix products, retain(): jnp.einsum('shd,shde->she', rot_query, prior_state, precision=lax.Precisi...  5.29 us
    add x1, other arithmetic, retain(): decays[None, :, None, None] * prior_state  4.3 us

profile of v2, /device:TPU:0, one launch (start us, length us, event | category | flops | bytes accessed | tf_op | source)
XLA Modules:
  0.0 89.5 jit_solution(16213107138339927080)
XLA Ops:
  0.6 0.7 convert_element_type.6
  1.3 0.1 dynamic_slice.3
  1.4 1.4 %select_reduce_fusion.gates = f32[16,16]{1,0:T(8,128)} fusion(f32[16,6]{0,1:T(8,128)} %param.33, s32[16,6]{0,1:T(8,128)} %param.32), kind=kLoop, calls=%fused_computation.11 | loop fusion | flops 4352 | bytes 1792 | tf_op jit(solution)/shard_map/reduce_sum | solution.py:500
  2.8 0.1 multiply_cosine_fusion
  2.9 30.5 %project.1 = (bf16[16,2048]{1,0:T(8,128)(2,1)}, f32[16,16,16]{2,1,0:T(8,128)}) custom-call(bf16[16,2048]{1,0:T(8,128)(2,1)} %tokens.3, f32[1,2048]{1,0:T(1,128)} %bitcast.13, bf16[128,512]{1,0:T(8,128)(2,1)} %weights_q.1, bf16[128,512]{1,0:T(8,128)(2,1)} %weights_k.1, bf16[128,512]{1,0:T(8,128)(2,1)} %weights_v.1, bf16[128,512]{1,0:T(8,128)(2,1)} %weights_g.1, ...), custom_call_target="tpu_custom_call" | custom-call | tf_op jit(solution)/shard_map/project/pallas_call | solution.py:506
  33.4 0.8 slice_convert_fusion.1
  34.1 0.1 reshape.131
  34.2 0.1 reshape.133
  34.3 0.1 reshape.129
  34.4 0.1 multiply_subtract_fusion
  34.5 0.1 pad_maximum_fusion
  34.6 5.3 %fusion.9 = f32[16,8,1,64]{3,2,1,0:T(1,128)S(1)} fusion(f32[16,8,64,1]{2,3,1,0:T(1,128)S(1)} %bitcast.11, f32[16,8,64,64]{3,2,1,0:T(8,128)} %param.22), kind=kOutput, calls=%fused_computation.31 | convolution fusion | flops 6291456 | bytes 2162688 | tf_op jit(solution)/shard_map/shd,shde->she/dot_general | solution.py:44
  39.9 0.2 multiply_reduce_fusion
  40.1 0.1 broadcast_multiply_fusion
  40.2 0.1 reshape.124
  40.3 1.3 %fusion.7.retained = bf16[16,512]{1,0:T(8,128)(2,1)} fusion(f32[16,512]{1,0:T(8,128)S(1)} %reshape.124, bf16[16,2048]{1,0:T(8,128)(2,1)} %get-tuple-element.4), kind=kLoop, calls=%fused_computation.20 | loop fusion | flops 57344 | bytes 65536 | tf_op jit(solution)/shard_map/convert_element_type | solution.py:57
  41.6 42.9 %layer.1 = bf16[16,2048]{1,0:T(8,128)(2,1)} custom-call(bf16[16,512]{1,0:T(8,128)(2,1)} %fusion.7.retained, bf16[16,2048]{1,0:T(8,128)(2,1)} %tokens.3, bf16[512,128]{1,0:T(8,128)(2,1)} %out_weight.1, f32[1,2048]{1,0:T(1,128)} %bitcast.14, f32[1,2048]{1,0:T(1,128)} %bitcast.15, f32[1,2048]{1,0:T(1,128)} %bitcast.16, ...), custom_call_target="tpu_custom_call" | custom-call | tf_op jit(solution)/shard_map/layer/pallas_call | solution.py:550
  84.6 0.0 copy-start
  84.6 4.3 %multiply_add_fusion = f32[16,8,64,64]{3,2,1,0:T(8,128)} fusion(f32[16,8,64,64]{3,2,1,0:T(8,128)} %param.22, f32[16,8,64]{2,1,0:T(8,128)S(1)} %reshape.133, f32[16,8,64]{2,1,0:T(8,128)S(1)} %get-tuple-element.20, f32[8]{0:T(128)S(1)} %dynamic_slice.3), kind=kLoop, calls=%fused_computation.1 | loop fusion | flops 1572864 | bytes 4259872 | tf_op jit(solution)/shard_map/add | solution.py:50
  88.9 0.0 copy-done
  88.9 0.6 copy.27
  (3 shorter events, 0.0 us)
Async XLA Ops:
  84.6 4.3 %copy-start = (bf16[16,2048]{1,0:T(8,128)(2,1)S(1)}, bf16[16,2048]{1,0:T(8,128)(2,1)}, u32[]{:S(2)}) copy-start(bf16[16,2048]{1,0:T(8,128)(2,1)} %layer.1) | copy-start | bytes 196612

commit v3 on v2

--- a/solution.py
+++ b/solution.py
@@ -16,45 +16,9 @@
 BF16 = jnp.bfloat16
 
 
-def rotate(vectors, lengths):
-    half_dim = vectors.shape[-1] // 2
-    frequency = THETA ** (-jnp.arange(half_dim, dtype=jnp.float32) / half_dim)
-    angles = lengths.astype(jnp.float32)[:, None] * frequency[None, :]
-    cosine = jnp.cos(angles)[:, None, :]
-    sine_part = jnp.sin(angles)[:, None, :]
-    leading = vectors[..., :half_dim]
-    trailing = vectors[..., half_dim:]
-    return jnp.concatenate(
-        [leading * cosine - trailing * sine_part, trailing * cosine + leading * sine_part], axis=-1
-    )
-
-
 def decay_table(head_count):
     head_order = jnp.arange(head_count, dtype=jnp.float32)
     return 1.0 - jnp.exp2(-5.0 - 7.0 * head_order / (head_count - 1))
-
-
-def retain(queries, keys_new, values, out_gate, prior_state, lengths, decays):
-    seq_count = queries.shape[0]
-    head_count = decays.shape[0]
-    layout = (seq_count, head_count, HEAD)
-    rot_query = rotate(queries.astype(jnp.float32).reshape(layout), lengths)
-    rot_key = rotate(keys_new.astype(jnp.float32).reshape(layout), lengths) * HEAD ** (-0.5)
-    wide_values = values.astype(jnp.float32).reshape(layout)
-    from_state = jnp.einsum(
-        "shd,shde->she", rot_query, prior_state, precision=lax.Precision.HIGHEST
-    )
-    self_term = jnp.sum(rot_query * rot_key, axis=-1, keepdims=True)
-    read_out = decays[None, :, None] * from_state + self_term * wide_values
-    new_state = (
-        decays[None, :, None, None] * prior_state
-        + rot_key[..., :, None] * wide_values[..., None, :]
-    )
-    normed = read_out * lax.rsqrt(jnp.mean(read_out * read_out, axis=-1, keepdims=True) + EPS)
-    gated_rows = normed.reshape(seq_count, head_count * HEAD) * jax.nn.silu(
-        out_gate.astype(jnp.float32)
-    )
-    return (gated_rows.astype(jnp.bfloat16), new_state)
 
 
 def norm_rows(wide, gain):
@@ -83,7 +47,7 @@
             return carry
 
         lax.fori_loop(1, total, body, 0)
-        pl.semaphore_wait(barrier, total - 1)
+        return lambda: pl.semaphore_wait(barrier, total - 1)
 
     def all_peers(self, source_of, target, send, recv):
         def body(i, carry):
@@ -189,17 +153,15 @@
     return sums, finish
 
 
-def project_kernel(
-    lows,
-    highs,
+def project(
+    place,
+    enter,
     tokens,
     gain,
-    weights_q,
-    weights_k,
-    weights_v,
-    weights_g,
-    gates,
-    projected,
+    routes,
+    route_gates,
+    weights,
+    weight_loads,
     gates_all,
     outgoing,
     features,
@@ -212,57 +174,123 @@
     near,
     far,
 ):
-    place = Place(lows, highs)
-    count = place.count
-    width = weights_q.shape[0]
-    cols = weights_q.shape[1]
+    lows, highs, count = place.lows, place.highs, place.count
+    _, width, cols = weights.shape
+    seqs = tokens.shape[0]
     normed = norm_rows(tokens[...].astype(F32), gain[...]).astype(BF16)
     for j in range(count):
         outgoing[j] = normed[:, j * width : (j + 1) * width]
-    place.greet()
+    features[place.lo, place.hi] = outgoing[place.ep]
+    lane = lax.broadcasted_iota(jnp.int32, (seqs, count), 1)
+    dense = jnp.zeros((seqs, count), F32)
+    for k in range(routes.shape[1]):
+        dense = dense + jnp.where(lane == routes[:, k : k + 1], route_gates[:, k : k + 1], 0.0)
+    own = place.lo * highs + place.hi
+    gates_all[own] = dense
+    enter()
     place.all_peers(
         lambda other: outgoing.at[other],
         features.at[place.lo, place.hi],
         sems.at[0],
         sems.at[1],
     )
-    features[place.lo, place.hi] = outgoing[place.ep]
-    place.all_peers(
-        lambda other: gates, gates_all.at[place.lo * highs + place.hi], sems.at[2], sems.at[3]
-    )
-    gates_all[place.lo * highs + place.hi] = gates[...]
+    for load in weight_loads:
+        load.wait()
     drain(outgoing.at[pl.ds(0, count - 1)], sems.at[1])
-    seqs = features.shape[2]
-    weights = (weights_q, weights_k, weights_v, weights_g)
 
     def fill(c):
         def multiply(l, carry):
             rows = features[l].reshape(highs * seqs, width)
-            piece = jnp.dot(rows, weights[c][...], preferred_element_type=F32).astype(BF16)
+            piece = jnp.dot(rows, weights[c], preferred_element_type=F32).astype(BF16)
             part[c, l] = piece.reshape(highs, seqs, cols)
             return carry
 
         lax.fori_loop(0, lows, multiply, 0)
 
     sums, finish = scatter_sums(place, fill, part, landed, halfway, last, send, near, far)
-    for c in range(4):
-        projected[:, c * cols : (c + 1) * cols] = sums[c].astype(BF16)
-    finish()
-    drain(outgoing.at[pl.ds(0, count - 1)], sems.at[0])
-    drain(gates_all.at[pl.ds(0, count - 1)], sems.at[3])
-    drain(gates_all.at[pl.ds(0, count - 1)], sems.at[2])
+    place.all_peers(lambda other: gates_all.at[own], gates_all.at[own], sems.at[2], sems.at[3])
+
+    def finish_all():
+        finish()
+        drain(outgoing.at[pl.ds(0, count - 1)], sems.at[0])
+        drain(gates_all.at[pl.ds(0, count - 1)], sems.at[2])
+
+    return [total.astype(BF16) for total in sums], finish_all
+
+
+def head_sums(values):
+    rows, cols = values.shape
+    pair = 2 * HEAD
+    row_of = lax.broadcasted_iota(jnp.int32, (pair, pair), 0) // HEAD
+    col_of = lax.broadcasted_iota(jnp.int32, (pair, pair), 1) // HEAD
+    ones = jnp.where(row_of == col_of, 1.0, 0.0).astype(F32)
+    groups = cols // pair
+    stacked = jnp.concatenate([values[:, g * pair : (g + 1) * pair] for g in range(groups)], axis=0)
+    summed = jnp.dot(
+        stacked, ones, preferred_element_type=F32, precision=lax.Precision.HIGHEST
+    )
+    return jnp.concatenate([summed[g * rows : (g + 1) * rows] for g in range(groups)], axis=1)
+
+
+def retain(place, projected, cosine, sine, state, turned, read):
+    queries, keys_new, values, out_gate = [member.astype(F32) for member in projected]
+    seqs, cols = queries.shape
+    lane = lax.broadcasted_iota(jnp.int32, (seqs, cols), 1)
+    leading = lax.rem(lane, HEAD) < HEAD // 2
+
+    def rotate(x):
+        swapped = jnp.where(
+            leading, pltpu.roll(x, cols - HEAD // 2, axis=1), pltpu.roll(x, HEAD // 2, axis=1)
+        )
+        return x * cosine[...] + swapped * sine[...]
+
+    rot_query = rotate(queries)
+    rot_key = rotate(keys_new) * HEAD ** (-0.5)
+    turned[...] = rot_query
+    pair = 2 * HEAD
+    deep = lax.broadcasted_iota(jnp.int32, (HEAD, pair), 0)
+    wide = lax.broadcasted_iota(jnp.int32, (HEAD, pair), 1)
+    picks = [wide == deep, wide == deep + HEAD]
+
+    def one_row(s, carry):
+        row = turned[pl.ds(s, 1), :]
+        for h in range(cols // HEAD):
+            both = row[:, (h // 2) * pair : (h // 2 + 1) * pair]
+            column = jnp.sum(
+                jnp.where(picks[h % 2], jnp.broadcast_to(both, (HEAD, pair)), 0.0),
+                axis=1,
+                keepdims=True,
+            )
+            read[h, pl.ds(s, 1), :] = jnp.sum(column * state[s, h], axis=0, keepdims=True)
+        return carry
+
+    lax.fori_loop(0, seqs, one_row, 0)
+    from_state = jnp.concatenate([read[h] for h in range(cols // HEAD)], axis=1)
+    head = (place.tp * (cols // HEAD) + lane // HEAD).astype(F32)
+    decays = 1.0 - jnp.exp2(-5.0 - 7.0 * head / (HEADS - 1))
+    read_out = decays * from_state + head_sums(rot_query * rot_key) * values
+    normed = read_out * lax.rsqrt(head_sums(read_out * read_out) / HEAD + EPS)
+    return (normed * jax.nn.silu(out_gate)).astype(BF16), rot_key
 
 
 def layer_kernel(
     lows,
     highs,
-    retained,
     tokens,
-    out_weight,
+    cosine,
+    sine,
+    routes,
+    route_gates,
+    mix_gain,
     post_gain,
     ffn_gain,
     out_gain,
-    gates_all,
+    prior_state,
+    query_weight,
+    key_weight,
+    value_weight,
+    gate_weight,
+    out_weight_far,
     expert_gate,
     expert_up,
     expert_down,
@@ -270,12 +298,26 @@
     shared_up,
     shared_down,
     result,
+    key_out,
+    value_out,
+    weights,
+    out_weight,
+    state,
     eg,
     eu,
     ed,
     sg,
     su,
     sd,
+    gates_all,
+    outgoing,
+    features,
+    first_part,
+    first_landed,
+    first_halfway,
+    first_last,
+    turned,
+    read,
     held,
     columns,
     mixed,
@@ -285,7 +327,6 @@
     hidden,
     shared_pair,
     give,
-    theirs,
     part,
     landed,
     halfway,
@@ -293,6 +334,10 @@
     pair,
     local_sems,
     sems,
+    first_sems,
+    first_send,
+    first_near,
+    first_far,
     held_send,
     held_near,
     held_far,
@@ -308,10 +353,17 @@
     place = Place(lows, highs)
     count = place.count
     twin = (place.ep, 1 - place.tp)
+    enter = place.greet()
     loads = [
         pltpu.make_async_copy(source, target, local_sems.at[i])
         for i, (source, target) in enumerate(
             (
+                (query_weight, weights.at[0]),
+                (key_weight, weights.at[1]),
+                (value_weight, weights.at[2]),
+                (gate_weight, weights.at[3]),
+                (prior_state, state),
+                (out_weight_far, out_weight),
                 (shared_gate, sg),
                 (shared_up, su),
                 (shared_down, sd),
@@ -323,12 +375,37 @@
     ]
     for load in loads:
         load.start()
-    place.greet()
     seqs, model = tokens.shape
     half = model // 2
     width = out_weight.shape[1]
-    held[place.lo, place.hi] = retained[...]
+    projected, finish_first = project(
+        place,
+        enter,
+        tokens,
+        mix_gain,
+        routes,
+        route_gates,
+        weights,
+        loads[:4],
+        gates_all,
+        outgoing,
+        features,
+        first_part,
+        first_landed,
+        first_halfway,
+        first_last,
+        first_sems,
+        first_send,
+        first_near,
+        first_far,
+    )
+    loads[4].wait()
+    retained, rot_key = retain(place, projected, cosine, sine, state, turned, read)
+    key_out[...] = rot_key
+    value_out[...] = projected[2]
+    held[place.lo, place.hi] = retained
     finish_held = gather_blocks(place, held, held_send, held_near, held_far)
+    loads[5].wait()
 
     def multiply(l, carry):
         rows = held[l].reshape(highs * seqs, held.shape[3])
@@ -354,8 +431,9 @@
 
     lax.fori_loop(1, 2 * count, send_back, 0)
     mixed[own_slot] = columns[place.lo * highs + place.hi]
-    for load in loads:
+    for load in loads[6:]:
         load.wait()
+    drain(gates_all.at[pl.ds(0, count - 1)], first_sems.at[3])
     drain(mixed.at[pl.ds(0, 2 * count - 1)], sems.at[1])
     mixed_sum = jnp.concatenate(
         [(mixed[e].astype(F32) + mixed[count + e].astype(F32)) for e in range(count)], axis=1
@@ -429,14 +507,14 @@
             return carry
 
         lax.fori_loop(0, steps, outward, 0)
-        start(give.at[c], theirs.at[c], sems.at[5], sum_twin.at[c], twin)
+        start(give.at[c], part.at[c], sems.at[5], sum_twin.at[c], twin)
 
     def fill(c):
-        drain(theirs.at[c], sum_twin.at[c])
+        drain(part.at[c], sum_twin.at[c])
 
         def inward(i, carry):
             piece = down(i, place.tp * half + c * cols)
-            other = theirs[c, pl.ds(i * chunk, chunk)].reshape(chunk_rows, cols).astype(F32)
+            other = part[c, pl.ds(i * chunk, chunk)].reshape(chunk_rows, cols).astype(F32)
             piece = (piece + other).astype(BF16)
             part[c, pl.ds(i * chunk, chunk)] = piece.reshape(chunk, highs, seqs, cols)
             return carry
@@ -454,6 +532,7 @@
     drain(pair.at[1 - place.tp], sems.at[7])
     mixture = jnp.concatenate([pair[0], pair[1]], axis=1)
     result[...] = (middle + norm_rows(mixture, out_gain[...])).astype(BF16)
+    finish_first()
     finish_held()
     finish_all()
     finish_sums()
@@ -495,70 +574,46 @@
     count = lows * highs
     seqs, model = tokens.shape
     width, local_cols = query_weight.shape
-    four = 4 * local_cols
-    experts = jnp.arange(count, dtype=jnp.int32)
-    gates = jnp.sum(
-        jnp.where(
-            routes[:, :, None] == experts[None, None, :], route_gates[:, :, None], jnp.float32(0)
+    heads_here = local_cols // HEAD
+    hidden_cols = expert_gate.shape[2]
+    shared_cols = shared_gate.shape[1]
+    half = model // 2
+    chunks = 4
+    steps = lows // max(1, min(lows, 256 // (highs * seqs)))
+    lane = jnp.arange(local_cols, dtype=jnp.int32)
+    half_dim = HEAD // 2
+    frequency = THETA ** (-(lane % half_dim).astype(F32) / half_dim)
+    angles = lengths.astype(F32)[:, None] * frequency[None, :]
+    cosine = jnp.cos(angles)
+    sine = jnp.where((lane % HEAD < half_dim)[None, :], -jnp.sin(angles), jnp.sin(angles))
+    result, rot_key, values = pl.pallas_call(
+        functools.partial(layer_kernel, lows, highs),
+        out_shape=(
+            jax.ShapeDtypeStruct((seqs, model), BF16),
+            jax.ShapeDtypeStruct((seqs, local_cols), F32),
+            jax.ShapeDtypeStruct((seqs, local_cols), BF16),
         ),
-        axis=1,
-    )
-    projected, gates_all = pl.pallas_call(
-        functools.partial(project_kernel, lows, highs),
-        out_shape=(
-            jax.ShapeDtypeStruct((seqs, four), BF16),
-            jax.ShapeDtypeStruct((count, seqs, count), F32),
-        ),
-        in_specs=[VM] * 7,
-        out_specs=(VM, VM),
+        in_specs=[VM] * 9 + [FAR] * 12,
+        out_specs=(VM, VM, VM),
         scratch_shapes=[
+            pltpu.VMEM((4, width, local_cols), BF16),
+            pltpu.VMEM((local_cols, width), BF16),
+            pltpu.VMEM(prior_state.shape, F32),
+            pltpu.VMEM((model, hidden_cols), BF16),
+            pltpu.VMEM((model, hidden_cols), BF16),
+            pltpu.VMEM((hidden_cols, model), BF16),
+            pltpu.VMEM((model, shared_cols), BF16),
+            pltpu.VMEM((model, shared_cols), BF16),
+            pltpu.VMEM((shared_cols, model), BF16),
+            pltpu.VMEM((count, seqs, count), F32),
             pltpu.VMEM((count, seqs, width), BF16),
             pltpu.VMEM((lows, highs, seqs, width), BF16),
             pltpu.VMEM((4, lows, highs, seqs, local_cols), BF16),
             pltpu.VMEM((4, lows, highs, seqs, local_cols), BF16),
             pltpu.VMEM((4, highs, seqs, local_cols), BF16),
             pltpu.VMEM((4, highs, seqs, local_cols), BF16),
-            pltpu.SemaphoreType.DMA((4,)),
-            pltpu.SemaphoreType.DMA((2,)),
-            pltpu.SemaphoreType.DMA((4,)),
-            pltpu.SemaphoreType.DMA((4,)),
-        ],
-        compiler_params=pltpu.CompilerParams(collective_id=0, has_side_effects=True),
-        name="project",
-    )(
-        tokens,
-        mix_gain.reshape(1, -1),
-        query_weight,
-        key_weight,
-        value_weight,
-        gate_weight,
-        gates,
-    )
-    queries, keys_new, values, out_gate = tuple(
-        projected[:, role * local_cols : (role + 1) * local_cols] for role in range(4)
-    )
-    heads_here = local_cols // HEAD
-    decays = lax.dynamic_slice_in_dim(
-        decay_table(HEADS), lax.axis_index("tp") * heads_here, heads_here, 0
-    )
-    retained, new_state = retain(queries, keys_new, values, out_gate, prior_state, lengths, decays)
-    hidden_cols = expert_gate.shape[2]
-    shared_cols = shared_gate.shape[1]
-    half = model // 2
-    chunks = 4
-    steps = lows // max(1, min(lows, 256 // (highs * seqs)))
-    result = pl.pallas_call(
-        functools.partial(layer_kernel, lows, highs),
-        out_shape=jax.ShapeDtypeStruct((seqs, model), BF16),
-        in_specs=[VM] * 7 + [FAR] * 6,
-        out_specs=VM,
-        scratch_shapes=[
-            pltpu.VMEM((model, hidden_cols), BF16),
-            pltpu.VMEM((model, hidden_cols), BF16),
-            pltpu.VMEM((hidden_cols, model), BF16),
-            pltpu.VMEM((model, shared_cols), BF16),
-            pltpu.VMEM((model, shared_cols), BF16),
-            pltpu.VMEM((shared_cols, model), BF16),
+            pltpu.VMEM((seqs, local_cols), F32),
+            pltpu.VMEM((heads_here, seqs, HEAD), F32),
             pltpu.VMEM((lows, highs, seqs, local_cols), BF16),
             pltpu.VMEM((count, seqs, width), BF16),
             pltpu.VMEM((2 * count, seqs, width), BF16),
@@ -570,12 +625,15 @@
             pltpu.VMEM((chunks, lows, highs, seqs, half // chunks), BF16),
             pltpu.VMEM((chunks, lows, highs, seqs, half // chunks), BF16),
             pltpu.VMEM((chunks, lows, highs, seqs, half // chunks), BF16),
-            pltpu.VMEM((chunks, lows, highs, seqs, half // chunks), BF16),
             pltpu.VMEM((chunks, highs, seqs, half // chunks), BF16),
             pltpu.VMEM((chunks, highs, seqs, half // chunks), BF16),
             pltpu.VMEM((2, seqs, half), F32),
-            pltpu.SemaphoreType.DMA((6,)),
+            pltpu.SemaphoreType.DMA((12,)),
             pltpu.SemaphoreType.DMA((8,)),
+            pltpu.SemaphoreType.DMA((4,)),
+            pltpu.SemaphoreType.DMA((2,)),
+            pltpu.SemaphoreType.DMA((4,)),
+            pltpu.SemaphoreType.DMA((4,)),
             pltpu.SemaphoreType.DMA((2,)),
             pltpu.SemaphoreType.DMA((highs,)),
             pltpu.SemaphoreType.DMA((highs,)),
@@ -588,22 +646,38 @@
             pltpu.SemaphoreType.DMA((chunks,)),
             pltpu.SemaphoreType.DMA((chunks,)),
         ],
-        compiler_params=pltpu.CompilerParams(collective_id=1, has_side_effects=True),
+        compiler_params=pltpu.CompilerParams(collective_id=0, has_side_effects=True),
         name="layer",
     )(
-        retained,
         tokens,
-        out_weight,
+        cosine,
+        sine,
+        routes,
+        route_gates,
+        mix_gain.reshape(1, -1),
         post_gain.reshape(1, -1),
         ffn_gain.reshape(1, -1),
         out_gain.reshape(1, -1),
-        gates_all,
+        prior_state,
+        query_weight,
+        key_weight,
+        value_weight,
+        gate_weight,
+        out_weight,
         expert_gate,
         expert_up,
         expert_down,
         shared_gate,
         shared_up,
         shared_down,
+    )
+    decays = lax.dynamic_slice_in_dim(
+        decay_table(HEADS), lax.axis_index("tp") * heads_here, heads_here, 0
+    )
+    layout = (seqs, heads_here, HEAD)
+    new_state = (
+        decays[None, :, None, None] * prior_state
+        + rot_key.reshape(layout)[..., :, None] * values.astype(F32).reshape(layout)[..., None, :]
     )
     return (result, new_state)
 

time: 89.8 us -> 83.7 us (0.932)
  matrix products: 5.29 us -> 0 us
  local copies, waits for them, and re-layouts: 1.02 us -> 5.06 us
  other arithmetic: 9.11 us -> 5.82 us
  Pallas kernels: 73.4 us -> 71.8 us
    dot_general x1 -> x0, matrix products: 5.29 us -> none  [retain(): jnp.einsum('shd,shde->she', rot_query, prior_state, precision=lax.Precisi...]
    unnamed x3 -> x5, local copies, waits for them, and re-layouts: 0.63 us -> 3.35 us
    mul x0 -> x2, local copies, waits for them, and re-layouts: none -> 1.64 us  [on_device(): rot_key.reshape(layout)[..., :, None]]
    pallas_call x2 -> x1, Pallas kernels: 73.4 us -> 71.8 us  [on_device(): pl.pallas_call(functools.partial(layer_kernel, lows, highs), out_shape=(j...]
    reduce_sum x1 -> x0, other arithmetic: 1.4 us -> none  [on_device(): jnp.sum(jnp.where(routes[:, :, None] == experts[None, None, :], route_gat...]
    convert_element_type x2 -> x1, other arithmetic: 2 us -> 0.66 us  [on_device(): angles = lengths.astype(F32)[:, None] * frequency[None, :]]
where the time goes in v3:
time: 83.7 us; the launch traced here: 83.4 us
  Pallas kernels  71.8 us (86%)
  other arithmetic  5.82 us (7%)
  local copies, waits for them, and re-layouts  5.06 us (6%)
    pallas_call x1, Pallas kernels, on_device(): pl.pallas_call(functools.partial(layer_kernel, lows, highs), out_shape=(j...  71.8 us
    add x1, other arithmetic, on_device(): decays[None, :, None, None] * prior_state  4.3 us
    unnamed x5, local copies, waits for them, and re-layouts  3.35 us

profile of v3, /device:TPU:0, one launch (start us, length us, event | category | flops | bytes accessed | tf_op | source)
XLA Modules:
  0.0 83.4 jit_solution(8842149156661554147)
XLA Ops:
  0.6 0.7 convert_element_type.11
  1.3 0.1 dynamic_slice.3
  1.4 1.4 %copy.22.routes = s32[16,6]{1,0:T(8,128)} copy(s32[16,6]{0,1:T(8,128)} %param.32) | data formatting | bytes 768 | tf_op args[12]
  2.8 1.4 %copy.23.route_gates = f32[16,6]{1,0:T(8,128)} copy(f32[16,6]{0,1:T(8,128)} %param.33) | data formatting | bytes 768 | tf_op args[13]
  4.1 0.8 negate_select_fusion
  4.9 71.8 %layer.1 = (bf16[16,2048]{1,0:T(8,128)(2,1)}, f32[16,512]{1,0:T(8,128)}, bf16[16,512]{1,0:T(8,128)(2,1)}) custom-call(bf16[16,2048]{1,0:T(8,128)(2,1)} %tokens.1, f32[16,512]{1,0:T(8,128)} %get-tuple-element.9.cosine, f32[16,512]{1,0:T(8,128)} %get-tuple-element.8.sine, s32[16,6]{1,0:T(8,128)} %copy.22.routes, f32[16,6]{1,0:T(8,128)} %copy.23.route_gates, ...), custom_call_target="tpu_custom_call" | custom-call | tf_op jit(solution)/shard_map/layer/pallas_call | solution.py:589
  76.8 0.8 %mul.51 = f32[16,8,64]{2,1,0:T(8,128)S(1)} reshape(f32[16,512]{1,0:T(8,128)} %get-tuple-element.6) | data formatting | bytes 65536 | tf_op jit(solution)/shard_map/mul | solution.py:680
  77.6 0.8 reshape.47
  78.4 0.0 copy-start
  78.4 4.3 %multiply_add_fusion = f32[16,8,64,64]{3,2,1,0:T(8,128)} fusion(f32[16,8,64,64]{3,2,1,0:T(8,128)} %prior_state.1, f32[16,8,64]{2,1,0:T(8,128)S(1)} %reshape.47, f32[16,8,64]{2,1,0:T(8,128)S(1)} %mul.51, f32[8]{0:T(128)S(1)} %dynamic_slice.3), kind=kLoop, calls=%fused_computation | loop fusion | flops 1572864 | bytes 4259872 | tf_op jit(solution)/shard_map/add | solution.py:679
  82.7 0.0 copy-done
  82.7 0.6 copy.25
  (3 shorter events, 0.0 us)
Async XLA Ops:
  78.4 4.3 %copy-start = (bf16[16,2048]{1,0:T(8,128)(2,1)S(1)}, bf16[16,2048]{1,0:T(8,128)(2,1)}, u32[]{:S(2)}) copy-start(bf16[16,2048]{1,0:T(8,128)(2,1)} %get-tuple-element.12) | copy-start | bytes 196612

commit v4 on v3

--- a/solution.py
+++ b/solution.py
@@ -114,16 +114,22 @@
     return finish
 
 
-def scatter_sums(place, fill, part, landed, halfway, last, send, near, far):
+def scatter_sums(place, fill, part, landed, halfway, last, crossed, met, end, send, near, far):
     lows, highs = place.lows, place.highs
-    chunks = part.shape[0]
-    for c in range(chunks):
+    plain = part.shape[0] - 1
+    fill(plain)
+    place.high_peers(
+        lambda other: part.at[plain, :, other], crossed.at[place.hi], send.at[2], far.at[plain]
+    )
+    crossed[place.hi] = part[plain, :, place.hi]
+    for c in range(plain):
         fill(c)
         place.low_peers(
             lambda other: part.at[c, other], landed.at[c, place.lo], send.at[0], near.at[c]
         )
         landed[c, place.lo] = part[c, place.lo]
-    for c in range(chunks):
+
+    def low_first(c):
         drain(landed.at[c, pl.ds(0, lows - 1)], near.at[c])
 
         def fold(h, carry):
@@ -138,17 +144,40 @@
             lambda other: halfway.at[c, other], last.at[c, place.hi], send.at[1], far.at[c]
         )
         last[c, place.hi] = halfway[c, place.hi]
+
+    for c in range(plain - 1):
+        low_first(c)
+    drain(crossed.at[pl.ds(0, highs - 1)], far.at[plain])
+
+    def fold_high(l, carry):
+        total = crossed[0, l].astype(F32)
+        for h in range(1, highs):
+            total = total + crossed[h, l].astype(F32)
+        met[l] = total.astype(BF16)
+        return carry
+
+    lax.fori_loop(0, lows, fold_high, 0)
+    place.low_peers(lambda other: met.at[other], end.at[place.lo], send.at[3], near.at[plain])
+    end[place.lo] = met[place.lo]
+    low_first(plain - 1)
     sums = []
-    for c in range(chunks):
+    for c in range(plain):
         drain(last.at[c, pl.ds(0, highs - 1)], far.at[c])
         total = last[c, 0].astype(F32)
         for h in range(1, highs):
             total = total + last[c, h].astype(F32)
         sums.append(total)
+    drain(end.at[pl.ds(0, lows - 1)], near.at[plain])
+    total = end[0].astype(F32)
+    for l in range(1, lows):
+        total = total + end[l].astype(F32)
+    sums.append(total)
 
     def finish():
-        drain(part.at[:, pl.ds(0, lows - 1)], send.at[0])
+        drain(part.at[pl.ds(0, plain), pl.ds(0, lows - 1)], send.at[0])
         drain(halfway.at[:, pl.ds(0, highs - 1)], send.at[1])
+        drain(crossed.at[pl.ds(0, highs - 1)], send.at[2])
+        drain(met.at[pl.ds(0, lows - 1)], send.at[3])
 
     return sums, finish
 
@@ -169,6 +198,9 @@
     landed,
     halfway,
     last,
+    crossed,
+    met,
+    end,
     sems,
     send,
     near,
@@ -181,13 +213,14 @@
     for j in range(count):
         outgoing[j] = normed[:, j * width : (j + 1) * width]
     features[place.lo, place.hi] = outgoing[place.ep]
-    lane = lax.broadcasted_iota(jnp.int32, (seqs, count), 1)
-    dense = jnp.zeros((seqs, count), F32)
-    for k in range(routes.shape[1]):
-        dense = dense + jnp.where(lane == routes[:, k : k + 1], route_gates[:, k : k + 1], 0.0)
+    expert = lax.broadcasted_iota(jnp.int32, (count, seqs), 0)
+    dense = jnp.zeros((count, seqs), F32)
+    for k in range(routes.shape[0]):
+        dense = dense + jnp.where(expert == routes[k : k + 1, :], route_gates[k : k + 1, :], 0.0)
     own = place.lo * highs + place.hi
-    gates_all[own] = dense
-    enter()
+    gates_all[own] = dense.T
+    with jax.named_scope("barrier"):
+        enter()
     place.all_peers(
         lambda other: outgoing.at[other],
         features.at[place.lo, place.hi],
@@ -196,7 +229,8 @@
     )
     for load in weight_loads:
         load.wait()
-    drain(outgoing.at[pl.ds(0, count - 1)], sems.at[1])
+    with jax.named_scope("wait_features"):
+        drain(outgoing.at[pl.ds(0, count - 1)], sems.at[1])
 
     def fill(c):
         def multiply(l, carry):
@@ -207,7 +241,10 @@
 
         lax.fori_loop(0, lows, multiply, 0)
 
-    sums, finish = scatter_sums(place, fill, part, landed, halfway, last, send, near, far)
+    with jax.named_scope("sum_projections"):
+        sums, finish = scatter_sums(
+            place, fill, part, landed, halfway, last, crossed, met, end, send, near, far
+        )
     place.all_peers(lambda other: gates_all.at[own], gates_all.at[own], sems.at[2], sems.at[3])
 
     def finish_all():
@@ -316,6 +353,9 @@
     first_landed,
     first_halfway,
     first_last,
+    first_crossed,
+    first_met,
+    first_end,
     turned,
     read,
     held,
@@ -331,6 +371,9 @@
     landed,
     halfway,
     last,
+    crossed,
+    met,
+    end,
     pair,
     local_sems,
     sems,
@@ -394,17 +437,27 @@
         first_landed,
         first_halfway,
         first_last,
+        first_crossed,
+        first_met,
+        first_end,
         first_sems,
         first_send,
         first_near,
         first_far,
     )
     loads[4].wait()
-    retained, rot_key = retain(place, projected, cosine, sine, state, turned, read)
-    key_out[...] = rot_key
-    value_out[...] = projected[2]
-    held[place.lo, place.hi] = retained
-    finish_held = gather_blocks(place, held, held_send, held_near, held_far)
+    with jax.named_scope("retain"):
+        retained, rot_key = retain(place, projected, cosine, sine, state, turned, read)
+        held[place.lo, place.hi] = retained
+
+    def emit():
+        values = projected[2].astype(F32)
+        for h in range(key_out.shape[1]):
+            key_out[:, h, :] = rot_key[:, h * HEAD : (h + 1) * HEAD]
+            value_out[:, h, :] = values[:, h * HEAD : (h + 1) * HEAD]
+
+    with jax.named_scope("gather_retained"):
+        finish_held = gather_blocks(place, held, held_send, held_near, held_far, emit)
     loads[5].wait()
 
     def multiply(l, carry):
@@ -434,7 +487,8 @@
     for load in loads[6:]:
         load.wait()
     drain(gates_all.at[pl.ds(0, count - 1)], first_sems.at[3])
-    drain(mixed.at[pl.ds(0, 2 * count - 1)], sems.at[1])
+    with jax.named_scope("wait_mixed"):
+        drain(mixed.at[pl.ds(0, 2 * count - 1)], sems.at[1])
     mixed_sum = jnp.concatenate(
         [(mixed[e].astype(F32) + mixed[count + e].astype(F32)) for e in range(count)], axis=1
     )
@@ -465,7 +519,8 @@
             twin,
         )
 
-    finish_all = gather_blocks(place, mine, all_send, all_near, all_far, shared, hand_over)
+    with jax.named_scope("gather_moe"):
+        finish_all = gather_blocks(place, mine, all_send, all_near, all_far, shared, hand_over)
 
     chunk = max(1, min(lows, 256 // (highs * seqs)))
     chunk_rows = chunk * highs * seqs
@@ -479,8 +534,10 @@
         up_sum[i] = jnp.dot(rows, eu[own_rows, :], preferred_element_type=F32)
         return carry
 
-    lax.fori_loop(0, steps, near_half, 0)
-    drain(normed_all.at[1 - place.tp], all_twin)
+    with jax.named_scope("near_half"):
+        lax.fori_loop(0, steps, near_half, 0)
+    with jax.named_scope("wait_twin"):
+        drain(normed_all.at[1 - place.tp], all_twin)
 
     def far_half(i, carry):
         rows = normed_all[1 - place.tp, pl.ds(i * chunk, chunk)].reshape(chunk_rows, half)
@@ -489,7 +546,8 @@
         hidden[i] = (jax.nn.silu(gate_cols) * up_cols).astype(BF16)
         return carry
 
-    lax.fori_loop(0, steps, far_half, 0)
+    with jax.named_scope("far_half"):
+        lax.fori_loop(0, steps, far_half, 0)
     cols = part.shape[4]
 
     def down(i, first):
@@ -499,7 +557,7 @@
         span = pl.ds(pl.multiple_of(first, cols), cols)
         return jnp.dot(hidden[i], ed[:, span], preferred_element_type=F32) * weight
 
-    for c in range(part.shape[0]):
+    for c in (part.shape[0] - 1, *range(part.shape[0] - 1)):
 
         def outward(i, carry):
             piece = down(i, (1 - place.tp) * half + c * cols).astype(BF16)
@@ -521,15 +579,17 @@
 
         lax.fori_loop(0, steps, inward, 0)
 
-    sums, finish_sums = scatter_sums(
-        place, fill, part, landed, halfway, last, sum_send, sum_near, sum_far
-    )
+    with jax.named_scope("sum_experts"):
+        sums, finish_sums = scatter_sums(
+            place, fill, part, landed, halfway, last, crossed, met, end, sum_send, sum_near, sum_far
+        )
     drain(shared_pair.at[2], sems.at[3])
     pair[place.tp] = jnp.concatenate(sums, axis=1) + (
         shared_pair[place.tp].astype(F32) + shared_pair[2].astype(F32)
     )
     start(pair.at[place.tp], pair.at[place.tp], sems.at[6], sems.at[7], twin)
-    drain(pair.at[1 - place.tp], sems.at[7])
+    with jax.named_scope("wait_pair"):
+        drain(pair.at[1 - place.tp], sems.at[7])
     mixture = jnp.concatenate([pair[0], pair[1]], axis=1)
     result[...] = (middle + norm_rows(mixture, out_gain[...])).astype(BF16)
     finish_first()
@@ -590,8 +650,8 @@
         functools.partial(layer_kernel, lows, highs),
         out_shape=(
             jax.ShapeDtypeStruct((seqs, model), BF16),
-            jax.ShapeDtypeStruct((seqs, local_cols), F32),
-            jax.ShapeDtypeStruct((seqs, local_cols), BF16),
+            jax.ShapeDtypeStruct((seqs, heads_here, HEAD), F32),
+            jax.ShapeDtypeStruct((seqs, heads_here, HEAD), F32),
         ),
         in_specs=[VM] * 9 + [FAR] * 12,
         out_specs=(VM, VM, VM),
@@ -609,9 +669,12 @@
             pltpu.VMEM((count, seqs, width), BF16),
             pltpu.VMEM((lows, highs, seqs, width), BF16),
             pltpu.VMEM((4, lows, highs, seqs, local_cols), BF16),
-            pltpu.VMEM((4, lows, highs, seqs, local_cols), BF16),
-            pltpu.VMEM((4, highs, seqs, local_cols), BF16),
-            pltpu.VMEM((4, highs, seqs, local_cols), BF16),
+            pltpu.VMEM((3, lows, highs, seqs, local_cols), BF16),
+            pltpu.VMEM((3, highs, seqs, local_cols), BF16),
+            pltpu.VMEM((3, highs, seqs, local_cols), BF16),
+            pltpu.VMEM((highs, lows, seqs, local_cols), BF16),
+            pltpu.VMEM((lows, seqs, local_cols), BF16),
+            pltpu.VMEM((lows, seqs, local_cols), BF16),
             pltpu.VMEM((seqs, local_cols), F32),
             pltpu.VMEM((heads_here, seqs, HEAD), F32),
             pltpu.VMEM((lows, highs, seqs, local_cols), BF16),
@@ -624,14 +687,17 @@
             pltpu.VMEM((3, seqs, half), BF16),
             pltpu.VMEM((chunks, lows, highs, seqs, half // chunks), BF16),
             pltpu.VMEM((chunks, lows, highs, seqs, half // chunks), BF16),
-            pltpu.VMEM((chunks, lows, highs, seqs, half // chunks), BF16),
-            pltpu.VMEM((chunks, highs, seqs, half // chunks), BF16),
-            pltpu.VMEM((chunks, highs, seqs, half // chunks), BF16),
+            pltpu.VMEM((chunks - 1, lows, highs, seqs, half // chunks), BF16),
+            pltpu.VMEM((chunks - 1, highs, seqs, half // chunks), BF16),
+            pltpu.VMEM((chunks - 1, highs, seqs, half // chunks), BF16),
+            pltpu.VMEM((highs, lows, seqs, half // chunks), BF16),
+            pltpu.VMEM((lows, seqs, half // chunks), BF16),
+            pltpu.VMEM((lows, seqs, half // chunks), BF16),
             pltpu.VMEM((2, seqs, half), F32),
             pltpu.SemaphoreType.DMA((12,)),
             pltpu.SemaphoreType.DMA((8,)),
             pltpu.SemaphoreType.DMA((4,)),
-            pltpu.SemaphoreType.DMA((2,)),
+            pltpu.SemaphoreType.DMA((4,)),
             pltpu.SemaphoreType.DMA((4,)),
             pltpu.SemaphoreType.DMA((4,)),
             pltpu.SemaphoreType.DMA((2,)),
@@ -641,7 +707,7 @@
             pltpu.SemaphoreType.DMA((highs,)),
             pltpu.SemaphoreType.DMA((highs,)),
             pltpu.SemaphoreType.DMA,
-            pltpu.SemaphoreType.DMA((2,)),
+            pltpu.SemaphoreType.DMA((4,)),
             pltpu.SemaphoreType.DMA((chunks,)),
             pltpu.SemaphoreType.DMA((chunks,)),
             pltpu.SemaphoreType.DMA((chunks,)),
@@ -652,8 +718,8 @@
         tokens,
         cosine,
         sine,
-        routes,
-        route_gates,
+        routes.T,
+        route_gates.T,
         mix_gain.reshape(1, -1),
         post_gain.reshape(1, -1),
         ffn_gain.reshape(1, -1),
@@ -674,10 +740,9 @@
     decays = lax.dynamic_slice_in_dim(
         decay_table(HEADS), lax.axis_index("tp") * heads_here, heads_here, 0
     )
-    layout = (seqs, heads_here, HEAD)
     new_state = (
         decays[None, :, None, None] * prior_state
-        + rot_key.reshape(layout)[..., :, None] * values.astype(F32).reshape(layout)[..., None, :]
+        + rot_key[..., :, None] * values[..., None, :]
     )
     return (result, new_state)
 

time: 83.7 us -> 76.5 us (0.914)
  local copies, waits for them, and re-layouts: 5.06 us -> 0.71 us
  Pallas kernels: 71.8 us -> 69.1 us
    pallas_call x1, Pallas kernels: 71.8 us -> 69.1 us  [on_device(): pl.pallas_call(functools.partial(layer_kernel, lows, highs), out_shape=(j...]
    unnamed x5 -> x3, local copies, waits for them, and re-layouts: 3.35 us -> 0.63 us
    mul x2 -> x0, local copies, waits for them, and re-layouts: 1.64 us -> none  [on_device(): rot_key.reshape(layout)[..., :, None]]
where the time goes in v4:
time: 76.5 us; the launch traced here: 76.3 us
  Pallas kernels  69.1 us (90%)
  other arithmetic  5.83 us (8%)
    pallas_call x1, Pallas kernels, on_device(): pl.pallas_call(functools.partial(layer_kernel, lows, highs), out_shape=(j...  69.1 us
    add x1, other arithmetic, on_device(): decays[None, :, None, None] * prior_state  4.31 us

profile of v4, /device:TPU:0, one launch (start us, length us, event | category | flops | bytes accessed | tf_op | source)
XLA Modules:
  0.0 76.3 jit_solution(17236397460309032712)
XLA Ops:
  0.6 0.7 convert_element_type.10
  1.3 0.1 dynamic_slice.3
  1.4 0.8 %negate_select_fusion = (f32[16,512]{1,0:T(8,128)}, f32[16,512]{1,0:T(8,128)}) fusion(f32[512]{0:T(512)S(1)} %fusion.3, f32[16]{0:T(128)S(1)} %convert_element_type.10, pred[512]{0:T(512)(128)(4,1)S(1)} %fusion.4), kind=kLoop, calls=%fused_computation.1 | loop fusion | flops 24576 | bytes 68160 | tf_op jit(solution)/shard_map/jit(_where)/select_n | solution.py:648
  2.2 69.1 %layer.1 = (bf16[16,2048]{1,0:T(8,128)(2,1)}, f32[16,8,64]{2,1,0:T(8,128)}, f32[16,8,64]{2,1,0:T(8,128)}) custom-call(bf16[16,2048]{1,0:T(8,128)(2,1)} %tokens.1, f32[16,512]{1,0:T(8,128)} %get-tuple-element.9.cosine, f32[16,512]{1,0:T(8,128)} %get-tuple-element.8.sine, s32[6,16]{1,0:T(8,128)} %bitcast.10, f32[6,16]{1,0:T(8,128)} %bitcast.11, ...), custom_call_target="tpu_custom_call" | custom-call | tf_op jit(solution)/shard_map/layer/pallas_call | solution.py:649
  71.3 0.0 copy-start
  71.3 4.3 %multiply_add_fusion = f32[16,8,64,64]{3,2,1,0:T(8,128)} fusion(f32[16,8,64,64]{3,2,1,0:T(8,128)} %prior_state.1, f32[16,8,64]{2,1,0:T(8,128)} %get-tuple-element.7, f32[16,8,64]{2,1,0:T(8,128)} %get-tuple-element.6, f32[8]{0:T(128)S(1)} %dynamic_slice.3), kind=kLoop, calls=%fused_computation | loop fusion | flops 1572864 | bytes 4259872 | tf_op jit(solution)/shard_map/add | solution.py:744
  75.7 0.0 copy-done
  75.7 0.6 copy.23
  (3 shorter events, 0.0 us)
Async XLA Ops:
  71.3 4.3 %copy-start = (bf16[16,2048]{1,0:T(8,128)(2,1)S(1)}, bf16[16,2048]{1,0:T(8,128)(2,1)}, u32[]{:S(2)}) copy-start(bf16[16,2048]{1,0:T(8,128)(2,1)} %get-tuple-element.12) | copy-start | bytes 196612

commit v5 on v4

--- a/solution.py
+++ b/solution.py
@@ -289,19 +289,22 @@
     wide = lax.broadcasted_iota(jnp.int32, (HEAD, pair), 1)
     picks = [wide == deep, wide == deep + HEAD]
 
-    def one_row(s, carry):
-        row = turned[pl.ds(s, 1), :]
-        for h in range(cols // HEAD):
-            both = row[:, (h // 2) * pair : (h // 2 + 1) * pair]
-            column = jnp.sum(
-                jnp.where(picks[h % 2], jnp.broadcast_to(both, (HEAD, pair)), 0.0),
-                axis=1,
-                keepdims=True,
-            )
-            read[h, pl.ds(s, 1), :] = jnp.sum(column * state[s, h], axis=0, keepdims=True)
+    together = 4
+
+    def some_rows(i, carry):
+        for s in [i * together + u for u in range(together)]:
+            row = turned[pl.ds(s, 1), :]
+            for h in range(cols // HEAD):
+                both = row[:, (h // 2) * pair : (h // 2 + 1) * pair]
+                column = jnp.sum(
+                    jnp.where(picks[h % 2], jnp.broadcast_to(both, (HEAD, pair)), 0.0),
+                    axis=1,
+                    keepdims=True,
+                )
+                read[h, pl.ds(s, 1), :] = jnp.sum(column * state[s, h], axis=0, keepdims=True)
         return carry
 
-    lax.fori_loop(0, seqs, one_row, 0)
+    lax.fori_loop(0, seqs // together, some_rows, 0)
     from_state = jnp.concatenate([read[h] for h in range(cols // HEAD)], axis=1)
     head = (place.tp * (cols // HEAD) + lane // HEAD).astype(F32)
     decays = 1.0 - jnp.exp2(-5.0 - 7.0 * head / (HEADS - 1))

time: 76.5 us -> 75.4 us (0.986)
  Pallas kernels: 69.1 us -> 68 us
    pallas_call x1, Pallas kernels: 69.1 us -> 68 us  [on_device(): pl.pallas_call(functools.partial(layer_kernel, lows, highs), out_shape=(j...]
where the time goes in v5:
time: 75.4 us; the launch traced here: 75.2 us
  Pallas kernels  68 us (90%)
  other arithmetic  5.83 us (8%)
    pallas_call x1, Pallas kernels, on_device(): pl.pallas_call(functools.partial(layer_kernel, lows, highs), out_shape=(j...  68 us
    add x1, other arithmetic, on_device(): decays[None, :, None, None] * prior_state  4.31 us

profile of v5, /device:TPU:0, one launch (start us, length us, event | category | flops | bytes accessed | tf_op | source)
XLA Modules:
  0.0 75.2 jit_solution(9344462662608142286)
XLA Ops:
  0.6 0.7 convert_element_type.10
  1.3 0.1 dynamic_slice.3
  1.4 0.8 %negate_select_fusion = (f32[16,512]{1,0:T(8,128)}, f32[16,512]{1,0:T(8,128)}) fusion(f32[512]{0:T(512)S(1)} %fusion.3, f32[16]{0:T(128)S(1)} %convert_element_type.10, pred[512]{0:T(512)(128)(4,1)S(1)} %fusion.4), kind=kLoop, calls=%fused_computation.1 | loop fusion | flops 24576 | bytes 68160 | tf_op jit(solution)/shard_map/jit(_where)/select_n | solution.py:651
  2.2 68.0 %layer.1 = (bf16[16,2048]{1,0:T(8,128)(2,1)}, f32[16,8,64]{2,1,0:T(8,128)}, f32[16,8,64]{2,1,0:T(8,128)}) custom-call(bf16[16,2048]{1,0:T(8,128)(2,1)} %tokens.1, f32[16,512]{1,0:T(8,128)} %get-tuple-element.9.cosine, f32[16,512]{1,0:T(8,128)} %get-tuple-element.8.sine, s32[6,16]{1,0:T(8,128)} %bitcast.10, f32[6,16]{1,0:T(8,128)} %bitcast.11, ...), custom_call_target="tpu_custom_call" | custom-call | tf_op jit(solution)/shard_map/layer/pallas_call | solution.py:652
  70.2 0.0 copy-start
  70.3 4.3 %multiply_add_fusion = f32[16,8,64,64]{3,2,1,0:T(8,128)} fusion(f32[16,8,64,64]{3,2,1,0:T(8,128)} %prior_state.1, f32[16,8,64]{2,1,0:T(8,128)} %get-tuple-element.7, f32[16,8,64]{2,1,0:T(8,128)} %get-tuple-element.6, f32[8]{0:T(128)S(1)} %dynamic_slice.3), kind=kLoop, calls=%fused_computation | loop fusion | flops 1572864 | bytes 4259872 | tf_op jit(solution)/shard_map/add | solution.py:747
  74.6 0.0 copy-done
  74.6 0.6 copy.23
  (3 shorter events, 0.0 us)
Async XLA Ops:
  70.2 4.3 %copy-start = (bf16[16,2048]{1,0:T(8,128)(2,1)S(1)}, bf16[16,2048]{1,0:T(8,128)(2,1)}, u32[]{:S(2)}) copy-start(bf16[16,2048]{1,0:T(8,128)(2,1)} %get-tuple-element.12) | copy-start | bytes 196612
